TPU v7x, 512 devices: a whole 4x8x8 slice. The times are simulated.
512 devices in a mesh: sp: 32 (over z, x), dp: 16 (over y, core).
Axes of the slice: x: 4, y: 8, z: 8, core: 2. Of those that a mesh axis runs over, the one named last changes fastest.
Arguments:
- inputs: bfloat16 [6144, 2048], P('sp'), may hold values from -6 to 6
- w_query: bfloat16 [2048, 2048], P('dp'), may hold values from -0.125 to 0.125
- w_key: bfloat16 [1024, 2048], P('dp'), may hold values from -0.125 to 0.125
- w_value: bfloat16 [1024, 2048], P('dp'), may hold values from -0.125 to 0.125
- query_gain: float32 [64], replicated, may hold values from 0.6 to 7
- key_gain: float32 [64], replicated, may hold values from 0.6 to 7
- grad_out: bfloat16 [6144, 2048], P('sp', 'dp'), may hold values from -6 to 6
Outputs:
- d_inputs: bfloat16 [6144, 2048], P('sp', 'dp')
- grad_wq: float32 [2048, 2048], P('dp')
- grad_wk: float32 [1024, 2048], P('dp')
- grad_wv: float32 [1024, 2048], P('dp')
All inputs are finite; a program needn't handle non-finite values.
Results may differ from a plain program's by a relative error of at most 0.019.
The roundings to bfloat16 on the way count: a program that leaves them out, or rounds other values in their place, can miss the bound.
Values may be sent and summed in bfloat16 or wider, within the bound.
A program may use at most 64 MiB of HBM per device.

v0:
```python
import jax
import jax.numpy as jnp
from jax import lax
from jax.sharding import Mesh
from jax.sharding import PartitionSpec as P

HEAD_WIDTH = 64
GRID_W = 64
SP = ("sp_0", "sp_1")


norm_eps = 1e-06
axial_base = 10000.0


def whole_of(shard, axes, dim):
    out = shard
    for number in range(len(axes) - 1, -1, -1):
        out = lax.all_gather(out, axes[number], axis=dim, tiled=True)
    return out


def in_blocks(shard, dim, length):
    before, after = (shard.shape[:dim], shard.shape[dim + 1 :])
    return jnp.moveaxis(shard.reshape(*before, length, -1, *after), dim, 0)


def summed_on_arrival(shard, axis, dim):
    length = lax.axis_size(axis)
    tiles = lax.all_to_all(in_blocks(shard, dim, length), axis, 0, 0, tiled=True)
    return jnp.sum(tiles, axis=0)


def sent_and_summed(shard, axis, dim):
    tiles = in_blocks(shard, dim, lax.axis_size(axis))
    arrived = lax.all_to_all(tiles, axis, split_axis=0, concat_axis=0, tiled=True)
    return arrived.astype(jnp.float32).sum(axis=0)


def packed_total(arrays, axis):
    ends = [0]
    for a in arrays:
        ends.append(ends[-1] + a.size)
    subtotal = lax.psum(jnp.concatenate([a.ravel() for a in arrays]), axis)
    return tuple((subtotal[b:e].reshape(a.shape) for a, b, e in zip(arrays, ends, ends[1:])))


def rotation_tables(offset, count):
    positions = offset + jnp.arange(count, dtype=jnp.int32)
    grid_rows = (positions // GRID_W).astype(jnp.float32)
    grid_cols = (positions % GRID_W).astype(jnp.float32)
    quarter = HEAD_WIDTH // 4
    freqs_axis = axial_base ** (-jnp.arange(quarter, dtype=jnp.float32) / quarter)
    angle_rows = grid_rows[:, None] * freqs_axis[None, :]
    angle_cols = grid_cols[:, None] * freqs_axis[None, :]
    cosine = jnp.concatenate(
        [jnp.cos(angle_rows), jnp.cos(angle_rows), jnp.cos(angle_cols), jnp.cos(angle_cols)], axis=1
    )
    sine = jnp.concatenate(
        [jnp.sin(angle_rows), jnp.sin(angle_rows), jnp.sin(angle_cols), jnp.sin(angle_cols)], axis=1
    )
    return (cosine, sine)


def quarter_turn(values):
    quarter = HEAD_WIDTH // 4
    return jnp.concatenate(
        [
            -values[..., quarter : 2 * quarter],
            values[..., :quarter],
            -values[..., 3 * quarter :],
            values[..., 2 * quarter : 3 * quarter],
        ],
        axis=-1,
    )


def quarter_back(values):
    quarter = HEAD_WIDTH // 4
    return jnp.concatenate(
        [
            values[..., quarter : 2 * quarter],
            -values[..., :quarter],
            values[..., 3 * quarter :],
            -values[..., 2 * quarter : 3 * quarter],
        ],
        axis=-1,
    )


def rotate(values, cosine, sine):
    return values * cosine + quarter_turn(values) * sine


def rotate_back(grads, cosine, sine):
    return grads * cosine + quarter_back(grads * sine)


def head_norm(raw):
    scale_inv = lax.rsqrt(jnp.mean(raw * raw, axis=-1, keepdims=True) + norm_eps)
    return (raw * scale_inv, scale_inv)


def head_norm_back(grads, normed, scale_inv, gain):
    scaled = grads * gain
    return scale_inv * (scaled - normed * jnp.mean(scaled * normed, axis=-1, keepdims=True))


def body(inputs, w_query, w_key, w_value, query_gain, key_gain, grad_out):
    tok_rows = inputs.shape[0]
    local_query = w_query.shape[0] // HEAD_WIDTH
    local_keys = w_key.shape[0] // HEAD_WIDTH
    group = local_query // local_keys
    key_width = local_keys * HEAD_WIDTH
    scale = HEAD_WIDTH ** (-0.5)
    contract = (((1,), (1,)), ((), ()))
    leading = (((0,), (0,)), ((), ()))
    offset = lax.axis_index(SP) * tok_rows
    cosine, sine = rotation_tables(offset, tok_rows)
    cos_wide = cosine[:, None, :]
    sin_wide = sine[:, None, :]
    q_raw = lax.dot_general(inputs, w_query, contract, preferred_element_type=jnp.float32).astype(
        jnp.bfloat16
    )
    w_pair = jnp.concatenate([w_key, w_value], axis=0)
    kv_raw = lax.dot_general(inputs, w_pair, contract, preferred_element_type=jnp.float32).astype(
        jnp.bfloat16
    )
    q_wide = (
        lax.optimization_barrier(q_raw)
        .astype(jnp.float32)
        .reshape(tok_rows, local_query, HEAD_WIDTH)
    )
    k_wide = (
        lax.optimization_barrier(kv_raw[:, :key_width])
        .astype(jnp.float32)
        .reshape(tok_rows, local_keys, HEAD_WIDTH)
    )
    q_normed, q_inv = head_norm(q_wide)
    k_normed, k_inv = head_norm(k_wide)
    q_rot = rotate(q_normed * query_gain, cos_wide, sin_wide).astype(jnp.bfloat16)
    k_rot = rotate(k_normed * key_gain, cos_wide, sin_wide).astype(jnp.bfloat16)
    kv_rot = jnp.concatenate([k_rot.reshape(tok_rows, key_width), kv_raw[:, key_width:]], axis=1)
    kv_every = whole_of(kv_rot, SP, 0)
    seq_rows = kv_every.shape[0]
    keys_every = kv_every[:, :key_width]
    values_every = kv_every[:, key_width:]
    grad_query = []
    log_totals = []
    deltas = []
    key_terms = [jnp.zeros((seq_rows, HEAD_WIDTH), jnp.float32)]
    value_terms = [jnp.zeros((seq_rows, HEAD_WIDTH), jnp.float32)]
    for member in range(local_query):
        kv_index = member // group
        query_head = q_rot[:, member, :]
        grad_head = grad_out[:, member * HEAD_WIDTH : (member + 1) * HEAD_WIDTH]
        scores = (
            lax.dot_general(query_head, keys_every, contract, preferred_element_type=jnp.float32)
            * scale
        )
        maxima = jnp.max(scores, axis=1, keepdims=True)
        log_total = maxima + jnp.log(jnp.sum(jnp.exp(scores - maxima), axis=1, keepdims=True))
        prob_exact = jnp.exp(scores - log_total)
        prob_half = prob_exact.astype(jnp.bfloat16)
        attn_rows = jnp.dot(prob_half, values_every, preferred_element_type=jnp.float32).astype(
            jnp.bfloat16
        )
        attn_wide = lax.optimization_barrier(attn_rows).astype(jnp.float32)
        delta_rows = jnp.sum(grad_head.astype(jnp.float32) * attn_wide, axis=1, keepdims=True)
        dprob = lax.dot_general(
            grad_head, values_every, contract, preferred_element_type=jnp.float32
        )
        dscore = (prob_exact * (dprob - delta_rows)).astype(jnp.bfloat16)
        grad_query.append(jnp.dot(dscore, keys_every, preferred_element_type=jnp.float32) * scale)
        log_totals.append(log_total)
        deltas.append(delta_rows)
        value_terms[kv_index] = value_terms[kv_index] + lax.dot_general(
            prob_half, grad_head, leading, preferred_element_type=jnp.float32
        )
        key_terms[kv_index] = (
            key_terms[kv_index]
            + lax.dot_general(dscore, query_head, leading, preferred_element_type=jnp.float32)
            * scale
        )
    gradient_query_rotated = jnp.stack(grad_query, axis=1)
    partial_sums = jnp.concatenate(key_terms + value_terms, axis=1)
    own_grads = summed_on_arrival(partial_sums, SP, 0)
    gradient_key_rotated = own_grads[:, :key_width].reshape(tok_rows, local_keys, HEAD_WIDTH)
    grad_q = head_norm_back(
        rotate_back(gradient_query_rotated, cos_wide, sin_wide), q_normed, q_inv, query_gain
    )
    grad_q = grad_q.reshape(tok_rows, local_query * HEAD_WIDTH).astype(jnp.bfloat16)
    grad_k = head_norm_back(
        rotate_back(gradient_key_rotated, cos_wide, sin_wide), k_normed, k_inv, key_gain
    )
    grad_kv = jnp.concatenate(
        [
            grad_k.reshape(tok_rows, key_width).astype(jnp.bfloat16),
            own_grads[:, key_width:].astype(jnp.bfloat16),
        ],
        axis=1,
    )
    head_part = jnp.dot(grad_q, w_query, preferred_element_type=jnp.float32)
    head_part = head_part + jnp.dot(grad_kv, w_pair, preferred_element_type=jnp.float32)
    d_inputs = sent_and_summed(head_part.astype(jnp.bfloat16), "dp", 1).astype(jnp.bfloat16)
    grad_wq = lax.dot_general(grad_q, inputs, leading, preferred_element_type=jnp.float32)
    grad_wkv = lax.dot_general(grad_kv, inputs, leading, preferred_element_type=jnp.float32)
    grad_wq, grad_wkv = packed_total((grad_wq, grad_wkv), SP)
    return (d_inputs, grad_wq, grad_wkv[:key_width], grad_wkv[key_width:])


def solution(mesh):
    finer = Mesh(mesh.devices.reshape(8, 4, mesh.shape["dp"]), ("sp_0", "sp_1", "dp"))
    return jax.shard_map(
        body,
        mesh=finer,
        in_specs=(P(SP, None), P("dp", None), P("dp", None), P("dp", None), P(), P(), P(SP, "dp")),
        out_specs=(P(SP, "dp"), P("dp", None), P("dp", None), P("dp", None)),
        check_vma=False,
    )
```

profile of v0, /device:TPU:16, one launch (start us, length us, event | category | flops | bytes accessed | tf_op | source)
XLA Modules:
  0.0 346.7 jit_solution(13979235363198071001)
XLA Ops:
  7.3 1.1 constant_dynamic-update-slice_fusion.1
  8.4 1.0 constant_dynamic-update-slice_fusion
  10.9 13.2 %all_gather.6 = bf16[768,128]{1,0:T(8,128)(2,1)} all-gather(bf16[192,128]{1,0:T(8,128)(2,1)S(1)} %copy.52), channel_id=1, replica_groups=mesh['sp_0'=8,'sp_1'=4,'dp'=16] {'sp_1'}, dimensions={0}, use_global_device_ids=true | all-gather | bytes 245760 | tf_op jit(solution)/shard_map/all_gather | solution.py:19
  26.5 44.7 %all-gather.2.cloned.1.call-done = bf16[6144,128]{1,0:T(8,128)(2,1)} async-done(((bf16[768,128]{1,0:T(8,128)(2,1)}), bf16[6144,128]{1,0:T(8,128)(2,1)}) %all-gather.2.cloned.1.call-update) | async-done | bytes 1572880 | tf_op jit(solution)/shard_map/all_gather | solution.py:19
  71.2 2.3 fusion.62
  73.6 0.8 exponential_reduce_fusion
  75.0 1.7 convolution_convert_fusion.2
  76.6 0.9 fusion.63
  78.4 1.0 fusion.50
  79.3 1.7 convolution_convert_fusion.3
  81.0 1.0 convolution_add_fusion
  82.0 1.5 fusion.5
  84.4 1.5 fusion.4
  87.4 1.9 pad_maximum_fusion
  89.4 3.5 %copy.59 = f32[6144,128]{1,0:T(8,128)} copy(f32[6144,128]{0,1:T(8,128)} %pad_maximum_fusion) | data formatting | bytes 6291456 | tf_op jit(solution)/shard_map/concatenate | solution.py:186
  92.9 7.1 %all-to-all-start = ((f32[32,192,128]{2,1,0:T(8,128)}), f32[32,192,128]{2,1,0:T(8,128)}, u32[]{:S(2)}, u32[]{:S(2)}) async-start(f32[32,192,128]{2,1,0:T(8,128)} %bitcast.89), calls=%async_computation | async-start | bytes 6291456 | tf_op jit(solution)/shard_map/all_to_all | solution.py:30
  100.0 1.2 mul.254
  101.3 1.3 mul.255
  102.5 1.3 mul.220
  103.9 1.6 copy.58
  105.5 2.7 fusion.12
  108.3 0.9 fusion.13
  109.5 0.9 multiply_convert_fusion
  111.1 57.8 %all-to-all-done = f32[32,192,128]{2,1,0:T(8,128)} async-done(((f32[32,192,128]{2,1,0:T(8,128)}), f32[32,192,128]{2,1,0:T(8,128)}, u32[]{:S(2)}, u32[]{:S(2)}) %all-to-all-start) | async-done | bytes 3145760 | tf_op jit(solution)/shard_map/all_to_all | solution.py:30
  168.9 2.0 reduce_sum.100
  172.0 1.5 pad_maximum_fusion.1
  174.4 27.8 %all_to_all.10 = bf16[16,192,128]{2,1,0:T(8,128)(2,1)S(1)} all-to-all(bf16[16,192,128]{2,1,0:T(8,128)(2,1)S(1)} %bitcast.92), channel_id=1, replica_groups=mesh['sp_0'=8,'sp_1'=4,'dp'=16] {'dp'}, dimensions={0} | all-to-all | bytes 1572864 | tf_op jit(solution)/shard_map/all_to_all | solution.py:36
  202.9 132.7 %all-reduce.2.cloned.1.call-done = f32[524288]{0:T(1024)} async-done(((f32[524288]{0:T(1024)}), f32[524288]{0:T(1024)}) %all-reduce.2.cloned.1.call-update) | async-done | bytes 2097168 | tf_op jit(solution)/shard_map/psum | solution.py:44
  335.6 1.4 fusion.58
  337.0 0.9 slice.158
  337.9 1.1 slice.154
  339.0 0.9 slice.156
  (125 shorter events, 11.0 us)
Async XLA Ops:
  7.2 2.2 copy-start
  7.2 2.7 copy-start.29
  7.2 16.9 %copy-start.5 = (bf16[128,2048]{1,0:T(8,128)(2,1)S(1)}, bf16[128,2048]{1,0:T(8,128)(2,1)}, u32[]{:S(2)}) copy-start(bf16[128,2048]{1,0:T(8,128)(2,1)} %param.8) | copy-start | bytes 1572868
  7.2 64.0 %all-gather.2.cloned.1.call-start = ((), (), s32[]{:S(2)}) async-start(), calls=%async_computation.2 | async-start | bytes 1769472 | tf_op jit(solution)/shard_map/all_gather | solution.py:19
  8.3 16.2 %copy-start.6 = (bf16[192,128]{1,0:T(8,128)(2,1)S(1)}, bf16[192,128]{1,0:T(8,128)(2,1)}, u32[]{:S(2)}) copy-start(bf16[192,128]{1,0:T(8,128)(2,1)} %param.13) | copy-start | bytes 147460
  9.3 16.9 %copy-start.31 = (f32[64]{0:T(128)S(1)}, f32[64]{0:T(128)}, u32[]{:S(2)}) copy-start(f32[64]{0:T(128)} %param.11) | copy-start | bytes 772
  9.8 15.5 %copy-start.8 = (bf16[192,64]{0,1:T(8,128)(2,1)}, bf16[192,64]{0,1:T(8,128)(2,1)S(1)}, u32[]{:S(2)}) copy-start(bf16[192,64]{0,1:T(8,128)(2,1)S(1)} %get-tuple-element.26) | copy-start | bytes 73732
  9.8 16.4 %copy-start.27 = (f32[192]{0:T(256)}, f32[192]{0:T(256)S(1)}, u32[]{:S(2)}) copy-start(f32[192]{0:T(256)S(1)} %add_rsqrt_fusion.1) | copy-start | bytes 2308
  10.2 16.1 %copy-start.17 = (f32[192,16]{0,1:T(8,128)}, f32[192,16]{0,1:T(8,128)S(1)}, u32[]{:S(2)}) copy-start(f32[192,16]{0,1:T(8,128)S(1)} %get-tuple-element.36) | copy-start | bytes 36868
  10.3 63.2 %copy-start.14 = (f32[192,64]{0,1:T(8,128)}, f32[192,64]{0,1:T(8,128)S(1)}, u32[]{:S(2)}) copy-start(f32[192,64]{0,1:T(8,128)S(1)} %get-tuple-element.30) | copy-start | bytes 147460
  24.5 1.8 copy-start.16
  26.2 47.4 %copy-start.12 = (f32[192,64]{0,1:T(8,128)}, f32[192,64]{0,1:T(8,128)S(1)}, u32[]{:S(2)}) copy-start(f32[192,64]{0,1:T(8,128)S(1)} %pad_maximum_fusion.4) | copy-start | bytes 147460
  26.3 47.3 %copy-start.25 = (f32[192,2]{0,1:T(2,128)}, f32[192,2]{0,1:T(2,128)S(1)}, u32[]{:S(2)}) copy-start(f32[192,2]{0,1:T(2,128)S(1)} %add_rsqrt_fusion) | copy-start | bytes 4612
  26.5 47.1 %copy-start.10 = (bf16[192,2,64]{0,2,1:T(8,128)(2,1)}, bf16[192,2,64]{0,2,1:T(8,128)(2,1)S(1)}, u32[]{:S(2)}) copy-start(bf16[192,2,64]{0,2,1:T(8,128)(2,1)S(1)} %fusion.23) | copy-start | bytes 147460
  73.5 1.4 copy-start.1
  75.0 1.7 copy-start.11
  81.0 1.0 copy-start.24
  83.6 2.4 copy-start.2
  86.0 1.5 copy-start.4
  92.9 76.0 %all-to-all-start = ((f32[32,192,128]{2,1,0:T(8,128)}), f32[32,192,128]{2,1,0:T(8,128)}, u32[]{:S(2)}, u32[]{:S(2)}) async-start(f32[32,192,128]{2,1,0:T(8,128)} %bitcast.89), calls=%async_computation | async-start | bytes 6291456 | tf_op jit(solution)/shard_map/all_to_all | solution.py:30
  100.0 235.7 %all-reduce.2.cloned.1.call-start = ((), (), s32[]{:S(2)}) async-start(), calls=%async_computation.3 | async-start | bytes 4194304 | tf_op jit(solution)/shard_map/psum | solution.py:44
  105.5 2.7 copy-start.3
  108.2 1.0 copy-start.15
  108.2 1.0 copy-start.26
  108.2 1.0 copy-start.32
  110.8 60.4 %copy-start.18 = (f32[192,16]{0,1:T(8,128)S(1)}, f32[192,16]{0,1:T(8,128)}, u32[]{:S(2)}) copy-start(f32[192,16]{0,1:T(8,128)} %copy-done.17) | copy-start | bytes 36868
  111.0 60.3 %copy-start.9 = (bf16[192,64]{0,1:T(8,128)(2,1)S(1)}, bf16[192,64]{0,1:T(8,128)(2,1)}, u32[]{:S(2)}) copy-start(bf16[192,64]{0,1:T(8,128)(2,1)} %copy-done.8) | copy-start | bytes 73732
  111.0 60.3 %copy-start.20 = (f32[192,16]{0,1:T(8,128)S(1)}, f32[192,16]{0,1:T(8,128)}, u32[]{:S(2)}) copy-start(f32[192,16]{0,1:T(8,128)} %copy-done.19) | copy-start | bytes 36868
  111.0 60.3 %copy-start.22 = (f32[192,16]{0,1:T(8,128)S(1)}, f32[192,16]{0,1:T(8,128)}, u32[]{:S(2)}) copy-start(f32[192,16]{0,1:T(8,128)} %copy-done.21) | copy-start | bytes 36868
  111.0 60.3 %copy-start.28 = (f32[192]{0:T(256)S(1)}, f32[192]{0:T(256)}, u32[]{:S(2)}) copy-start(f32[192]{0:T(256)} %copy-done.27) | copy-start | bytes 2308
  111.1 60.3 %copy-start.30 = (f32[64]{0:T(128)S(1)}, f32[64]{0:T(128)}, u32[]{:S(2)}) copy-start(f32[64]{0:T(128)} %param.12) | copy-start | bytes 772
  335.6 2.2 slice-start
  (5 other events, 3.7 us)
Sparse Core Ops, SparseCore 0:
  24.3 46.8 all-gather.1
  173.6 162.0 all-reduce.1
where the time goes:
time: 348 us; the launch traced here: 347 us
  waiting for transfers between devices  235 us (68%)
  blocking collectives  41 us (12%)
  local copies, waits for them, and re-layouts  20.2 us (6%)
  matrix products  18.5 us (5%)
  between operations  14.8 us (4%)
  other arithmetic  9.69 us (3%)
  starting transfers between devices  7.18 us (2%)
    psum x1, waiting for transfers between devices, packed_total(): subtotal = lax.psum(jnp.concatenate([a.ravel() for a in arrays]), axis)  133 us
    all_to_all x1, waiting for transfers between devices, summed_on_arrival(): lax.all_to_all(in_blocks(shard, dim, length), axis, 0, 0, tiled=True)  57.8 us
    all_gather x1, waiting for transfers between devices, whole_of(): out = lax.all_gather(out, axes[number], axis=dim, tiled=True)  44.7 us
    all_to_all x1, blocking collectives, sent_and_summed(): lax.all_to_all(tiles, axis, split_axis=0, concat_axis=0, tiled=True)  27.8 us
    all_gather x1, blocking collectives, whole_of(): out = lax.all_gather(out, axes[number], axis=dim, tiled=True)  13.2 us
    all_to_all x1, starting transfers between devices, summed_on_arrival(): lax.all_to_all(in_blocks(shard, dim, length), axis, 0, 0, tiled=True)  7.1 us
  transfers between devices with their start and end apart: 3, of which 3 were waited for; matrix products, arithmetic and copies ran while one was open for 4% of the time, Pallas kernels for 0%

commit v1 on v0

v1 whole, which is shorter than its diff:
```python
import functools

import jax
import jax.numpy as jnp
import numpy as np
from jax import lax
from jax.experimental import pallas as pl
from jax.experimental.pallas import tpu as pltpu
from jax.sharding import Mesh
from jax.sharding import PartitionSpec as P

HEAD_WIDTH = 64
GRID_W = 64
GROUP = 2
LANES = 128
MESH = pl.DeviceIdType.MESH
F32 = jnp.float32
BF16 = jnp.bfloat16

norm_eps = 1e-06
axial_base = 10000.0

NT = (((1,), (1,)), ((), ()))
NN = (((1,), (0,)), ((), ()))
TN = (((0,), (0,)), ((), ()))


def dot(a, b, dims):
    return lax.dot_general(a, b, dims, preferred_element_type=F32)


def rotation_constants(grid_rows):
    quarter = HEAD_WIDTH // 4
    freqs = axial_base ** (-np.arange(quarter, dtype=np.float64) / quarter)
    by_row = np.arange(grid_rows, dtype=np.float64)[:, None] * freqs
    by_col = np.arange(GRID_W, dtype=np.float64)[:, None] * freqs

    def wide(first, second):
        head = np.concatenate([first, first, second, second], axis=1)
        return np.concatenate([head, head], axis=1)

    none_r, none_c = np.zeros_like(by_row), np.zeros_like(by_col)
    rows = np.stack([wide(np.cos(by_row), none_r), wide(np.sin(by_row), none_r)])
    cols = np.stack([wide(none_c, np.cos(by_col)), wide(none_c, np.sin(by_col))])
    return rows.astype(np.float32), cols.astype(np.float32)


def farthest_first(n):
    return sorted(range(1, n), key=lambda d: -min(d, n - d))


def nearest_first(n):
    return sorted(range(1, n), key=lambda d: min(d, n - d))


def kernel(
    sizes, x_ref, wq_ref, wk_ref, wv_ref, qg_ref, kg_ref, do_ref, rows_ref, cols_ref,
    din_ref, gw_ref,
    w_all, x_buf, kv_buf, q_buf, do_buf, qa, doa, e_buf, dp_buf, stat, cfac, delta, st_buf,
    dqt, dq_all, dkv_send, dkv_buf, dq_send, dq_buf, g_buf, xin, hp_send, hp_buf, gw_part, gwr_buf,
    load_sem, kv_ss, kv_rs, q_ss, q_rs, do_ss, do_rs, st_ss, st_rs, xin_ss, xin_rs, dkv_ss, dkv_rs,
    dq_ss, dq_rs, g_ss, g_rs, hp_ss, hp_rs, gwr_ss, gwr_rs, agz_ss, agz_rs, agx_ss, agx_rs,
):
    Z, X, Y, C, T, D, R, CH = sizes
    DX = D // X
    DC = D // (Y * C)
    WR = w_all.shape[0]
    PZ = WR // Z
    z, x, y, c = (lax.axis_index(a) for a in ("z", "x", "y", "c"))

    def on_z(d):
        return {"z": lax.rem(z + d, Z)}

    def on_x(d):
        return {"x": lax.rem(x + d, X)}

    def on_dp(dy, dc):
        return {"y": lax.rem(y + dy, Y), "c": lax.rem(c + dc, C)}

    def remote(src, dst, ss, rs, dev):
        return pltpu.make_async_remote_copy(
            src_ref=src, dst_ref=dst, send_sem=ss, recv_sem=rs, device_id=dev, device_id_type=MESH
        )

    dp_pairs = [(dy, dc) for dy in [0] + nearest_first(Y) for dc in range(C) if (dy, dc) != (0, 0)]

    nq, nk = wq_ref.shape[0], wk_ref.shape[0]
    loads = [
        pltpu.make_async_copy(x_ref, x_buf, load_sem.at[0]),
        pltpu.make_async_copy(wq_ref, w_all.at[pl.ds(0, nq)], load_sem.at[1]),
        pltpu.make_async_copy(wk_ref, w_all.at[pl.ds(nq, nk)], load_sem.at[2]),
        pltpu.make_async_copy(wv_ref, w_all.at[pl.ds(nq + nk, nk)], load_sem.at[3]),
        pltpu.make_async_copy(do_ref, do_buf.at[x], load_sem.at[4]),
    ]
    for load in loads:
        load.start()
    barrier = pltpu.get_barrier_semaphore()
    for d in range(1, Z):
        pl.semaphore_signal(barrier, inc=1, device_id=on_z(d), device_id_type=MESH)
    for d in range(1, X):
        pl.semaphore_signal(barrier, inc=1, device_id=on_x(d), device_id_type=MESH)
    for dy, dc in dp_pairs:
        pl.semaphore_signal(barrier, inc=1, device_id=on_dp(dy, dc), device_id_type=MESH)

    lane = lax.broadcasted_iota(jnp.int32, (T, LANES), 1)
    low = lax.rem(lane, 32) < 16
    head0 = lane < HEAD_WIDTH
    n_rows = T // GRID_W
    first_row = (z * X + x) * n_rows

    def table(k):
        return jnp.concatenate(
            [rows_ref[k, pl.ds(first_row + j, 1), :] + cols_ref[k] for j in range(n_rows)], axis=0
        )

    cos = table(0)
    sin = table(1)
    sin = jnp.where(low, -sin, sin)

    def turned(v):
        return jnp.where(low, pltpu.roll(v, LANES - 16, 1), pltpu.roll(v, 16, 1))

    def rotate(v):
        return v * cos + turned(v) * sin

    def rotate_back(v):
        return v * cos - turned(v) * sin

    def head_mean(v):
        first = jnp.sum(jnp.where(head0, v, 0.0), axis=1, keepdims=True)
        second = jnp.sum(jnp.where(head0, 0.0, v), axis=1, keepdims=True)
        return jnp.where(head0, first, second) * (1.0 / HEAD_WIDTH)

    qg = jnp.concatenate([qg_ref[...], qg_ref[...]], axis=1)
    kg = jnp.concatenate([kg_ref[...], kg_ref[...]], axis=1)

    for load in loads:
        load.wait()
    raw = dot(x_buf[...], w_all[...], NT).astype(BF16).astype(F32)
    q_raw = raw[:, :LANES]
    kv_raw = raw[:, LANES:]
    q_inv = lax.rsqrt(head_mean(q_raw * q_raw) + norm_eps)
    q_hat = q_raw * q_inv
    k_inv = lax.rsqrt(head_mean(kv_raw * kv_raw) + norm_eps)
    k_hat = kv_raw * k_inv
    q_buf[x] = rotate(q_hat * qg).astype(BF16)
    kv_buf[0] = jnp.where(head0, rotate(k_hat * kg), kv_raw).astype(BF16)

    pl.semaphore_wait(barrier, (Z - 1) + (X - 1) + len(dp_pairs))

    kv_copies, q_copies, do_copies = {}, {}, {}
    for d in nearest_first(Z):
        kv_copies[d] = remote(kv_buf.at[0], kv_buf.at[d], kv_ss.at[d], kv_rs.at[d], on_z(d))
        kv_copies[d].start()
    for d in nearest_first(X):
        q_copies[d] = remote(q_buf.at[x], q_buf.at[x], q_ss.at[d], q_rs.at[d], on_x(d))
        q_copies[d].start()
        do_copies[d] = remote(do_buf.at[x], do_buf.at[x], do_ss.at[d], do_rs.at[d], on_x(d))
        do_copies[d].start()
    for d in range(1, X):
        q_copies[d].wait()
        do_copies[d].wait()

    q_rows = q_buf[...].reshape(X * T, LANES).astype(F32) * (HEAD_WIDTH**-0.5)
    do_rows = do_buf[...].reshape(X * T, LANES).astype(F32)
    keep = lax.broadcasted_iota(jnp.int32, (X * T, LANES), 1) < HEAD_WIDTH
    half = R // GROUP
    qa[0:half] = jnp.where(keep, q_rows, 0.0).astype(BF16).reshape(half, CH, LANES)
    qa[half:] = (
        jnp.where(keep, pltpu.roll(q_rows, HEAD_WIDTH, 1), 0.0).astype(BF16).reshape(half, CH, LANES)
    )
    doa[0:half] = (
        jnp.where(keep, 0.0, pltpu.roll(do_rows, HEAD_WIDTH, 1)).astype(BF16).reshape(half, CH, LANES)
    )
    doa[half:] = jnp.where(keep, 0.0, do_rows).astype(BF16).reshape(half, CH, LANES)

    for d in [0] + nearest_first(Z):
        if d:
            kv_copies[d].wait()

        def forward(r, carry, d=d):
            kv = kv_buf[d]
            s = dot(kv, qa[r], NT)
            dp = dot(kv, doa[r], NT)
            m = jnp.max(s, axis=0, keepdims=True)
            e = jnp.exp(s - m)
            stat[d, 0, r] = m
            stat[d, 1, r] = jnp.sum(e, axis=0, keepdims=True)
            stat[d, 2, r] = jnp.sum(e * dp, axis=0, keepdims=True)
            e_buf[d, r] = e
            dp_buf[d, r] = dp
            return carry

        lax.fori_loop(0, R, forward, 0)

    top = stat[0, 0]
    for d in range(1, Z):
        top = jnp.maximum(top, stat[d, 0])
    total = jnp.zeros_like(top)
    weighted = jnp.zeros_like(top)
    for d in range(Z):
        f = jnp.exp(stat[d, 0] - top)
        total = total + stat[d, 1] * f
        weighted = weighted + stat[d, 2] * f
    st_buf[0, 0] = top
    st_buf[0, 1] = total
    st_buf[0, 2] = weighted
    st_copies = {}
    for d in nearest_first(X):
        st_copies[d] = remote(st_buf.at[0], st_buf.at[d], st_ss.at[d], st_rs.at[d], on_x(d))
        st_copies[d].start()
    xin_copies = {}
    for d in nearest_first(X):
        cols = pl.multiple_of(lax.rem(x + d, X) * DX, LANES)
        xin_copies[d] = remote(
            x_buf.at[:, pl.ds(cols, DX)], xin.at[d], xin_ss.at[d], xin_rs.at[d], on_x(d)
        )
        xin_copies[d].start()
    for d in range(1, X):
        st_copies[d].wait()
    top = st_buf[0, 0]
    for d in range(1, X):
        top = jnp.maximum(top, st_buf[d, 0])
    total = jnp.zeros_like(top)
    weighted = jnp.zeros_like(top)
    for d in range(X):
        f = jnp.exp(st_buf[d, 0] - top)
        total = total + st_buf[d, 1] * f
        weighted = weighted + st_buf[d, 2] * f
    log_total = top + jnp.log(total)
    delta[...] = weighted / total
    for d in range(Z):
        cfac[d] = jnp.exp(stat[d, 0] - log_total)

    dqt[...] = jnp.zeros_like(dqt)
    dkv_copies = {}
    dkv_own = None
    for d in farthest_first(Z) + [0]:
        k_t = kv_buf[d].astype(F32).T[:HEAD_WIDTH].astype(BF16)

        def backward(r, acc, d=d, k_t=k_t):
            p = e_buf[d, r] * cfac[d, r]
            ds = (p * (dp_buf[d, r] - delta[r])).astype(BF16)
            acc = acc + dot(p.astype(BF16), doa[r], NN) + dot(ds, qa[r], NN)
            dqt[r] += dot(k_t, ds, NN)
            return acc

        acc = lax.fori_loop(0, R, backward, jnp.zeros((T, LANES), F32))
        if d:
            dkv_send[d] = acc.astype(BF16)
            dkv_copies[d] = remote(
                dkv_send.at[d], dkv_buf.at[d], dkv_ss.at[d], dkv_rs.at[d], on_z(Z - d)
            )
            dkv_copies[d].start()
        else:
            dkv_own = acc

    dq_rows = jnp.concatenate(
        [jnp.concatenate([dqt[r], dqt[half + r]], axis=0).T for r in range(half)], axis=0
    )
    dq_all[...] = dq_rows.reshape(X, T, LANES)
    dq_send[...] = dq_rows.astype(BF16).reshape(X, T, LANES)
    dq_copies = {}
    for d in range(1, X):
        dq_copies[d] = remote(
            dq_send.at[lax.rem(x + X - d, X)], dq_buf.at[d], dq_ss.at[d], dq_rs.at[d], on_x(X - d)
        )
        dq_copies[d].start()
    dq_own = dq_all[x]
    for d in range(1, X):
        dq_copies[d].wait()
        dq_own = dq_own + dq_buf[d].astype(F32)
    for d in range(1, Z):
        dkv_copies[d].wait()
        dkv_own = dkv_own + dkv_buf[d].astype(F32)

    def norm_back(grads, normed, inv, gain):
        u = rotate_back(grads) * gain
        return inv * (u - normed * head_mean(u * normed))

    grad_q = norm_back(dq_own * (HEAD_WIDTH**-0.5), q_hat, q_inv, qg)
    grad_k = norm_back(jnp.where(head0, dkv_own, 0.0), k_hat, k_inv, kg)
    grad_kv = jnp.where(head0, grad_k, dkv_own)
    g = jnp.concatenate([grad_q.astype(BF16), grad_kv.astype(BF16)], axis=1)
    g_buf[0] = g
    g_copies = {}
    for d in nearest_first(X):
        g_copies[d] = remote(g_buf.at[0], g_buf.at[d], g_ss.at[d], g_rs.at[d], on_x(d))
        g_copies[d].start()

    def part_for(dy, dc):
        j = lax.rem(y + dy, Y) * C + lax.rem(c + dc, C)
        return dot(g, w_all[:, pl.ds(pl.multiple_of(j * DC, LANES), DC)], NN).astype(BF16)

    hp_copies = {}
    for dy, dc in reversed(dp_pairs):
        slot = dy * C + dc
        hp_send[slot] = part_for(dy, dc)
        hp_copies[slot] = remote(
            hp_send.at[slot], hp_buf.at[slot], hp_ss.at[slot], hp_rs.at[slot], on_dp(dy, dc)
        )
        hp_copies[slot].start()
    din = part_for(0, 0).astype(F32)

    cols = pl.multiple_of(x * DX, LANES)
    gw = dot(g, x_buf[:, pl.ds(cols, DX)], TN)
    for d in range(1, X):
        g_copies[d].wait()
        xin_copies[d].wait()
        gw = gw + dot(g_buf[d], xin[d], TN)
    gw_part[...] = gw.astype(BF16)
    gwr_copies = {}
    for d in farthest_first(Z):
        rows = pl.multiple_of(lax.rem(z + d, Z) * PZ, PZ)
        gwr_copies[d] = remote(
            gw_part.at[pl.ds(rows, PZ)], gwr_buf.at[d], gwr_ss.at[d], gwr_rs.at[d], on_z(d)
        )
        gwr_copies[d].start()
    my_rows = pl.multiple_of(z * PZ, PZ)
    piece = gw_part[pl.ds(my_rows, PZ), :].astype(F32)
    for d in range(1, Z):
        gwr_copies[d].wait()
        piece = piece + gwr_buf[d].astype(F32)
    gw_ref[pl.ds(my_rows, PZ), pl.ds(cols, DX)] = piece.astype(BF16)

    def region(dz):
        rows = pl.multiple_of(lax.rem(z + Z - dz, Z) * PZ, PZ)
        return gw_ref.at[pl.ds(rows, PZ), pl.ds(cols, DX)]

    agz_copies, agx_copies = {}, {}
    own = region(0)
    for d in nearest_first(Z):
        agz_copies[d] = remote(own, own, agz_ss.at[d], agz_rs.at[d], on_z(d))
        agz_copies[d].start()
    for dz in [0] + nearest_first(Z):
        if dz:
            agz_copies[dz].wait_recv()
        block = region(dz)
        for d in nearest_first(X):
            agx_copies[dz, d] = remote(
                block, block, agx_ss.at[d, dz], agx_rs.at[d, dz], on_x(d)
            )
            agx_copies[dz, d].start()

    for slot, copy in hp_copies.items():
        copy.wait()
        din = din + hp_buf[slot].astype(F32)
    din_ref[...] = din.astype(BF16)
    for copy in agx_copies.values():
        copy.wait()
    for copy in agz_copies.values():
        copy.wait_send()


def make_body(Z, X, Y, C):
    def body(inputs, w_query, w_key, w_value, query_gain, key_gain, grad_out):
        T, D = inputs.shape
        nq, nk = w_query.shape[0], w_key.shape[0]
        per_head = X * T
        CH = 256 if per_head % 256 == 0 else 384
        R = GROUP * per_head // CH
        rows, cols = rotation_constants(Z * X * T // GRID_W)
        DX, DC, PZ = D // X, D // (Y * C), (nq + 2 * nk) // Z
        sizes = (Z, X, Y, C, T, D, R, CH)
        dma = pltpu.SemaphoreType.DMA
        pair = lambda *n: [dma(n), dma(n)]
        vmem = pl.BlockSpec(memory_space=pltpu.VMEM)
        hbm = pl.BlockSpec(memory_space=pl.ANY)
        din, gw = pl.pallas_call(
            functools.partial(kernel, sizes),
            out_shape=(
                jax.ShapeDtypeStruct((T, DC), BF16),
                jax.ShapeDtypeStruct((nq + 2 * nk, D), BF16),
            ),
            in_specs=[hbm, hbm, hbm, hbm, vmem, vmem, hbm, vmem, vmem],
            out_specs=(vmem, vmem),
            scratch_shapes=[
                pltpu.VMEM((nq + 2 * nk, D), BF16),
                pltpu.VMEM((T, D), BF16),
                pltpu.VMEM((Z, T, LANES), BF16),
                pltpu.VMEM((X, T, LANES), BF16),
                pltpu.VMEM((X, T, LANES), BF16),
                pltpu.VMEM((R, CH, LANES), BF16),
                pltpu.VMEM((R, CH, LANES), BF16),
                pltpu.VMEM((Z, R, T, CH), F32),
                pltpu.VMEM((Z, R, T, CH), F32),
                pltpu.VMEM((Z, 3, R, 1, CH), F32),
                pltpu.VMEM((Z, R, 1, CH), F32),
                pltpu.VMEM((R, 1, CH), F32),
                pltpu.VMEM((X, 3, R, 1, CH), F32),
                pltpu.VMEM((R, HEAD_WIDTH, CH), F32),
                pltpu.VMEM((X, T, LANES), F32),
                pltpu.VMEM((Z, T, LANES), BF16),
                pltpu.VMEM((Z, T, LANES), BF16),
                pltpu.VMEM((X, T, LANES), BF16),
                pltpu.VMEM((X, T, LANES), BF16),
                pltpu.VMEM((X, T, nq + 2 * nk), BF16),
                pltpu.VMEM((X, T, DX), BF16),
                pltpu.VMEM((Y * C, T, DC), BF16),
                pltpu.VMEM((Y * C, T, DC), BF16),
                pltpu.VMEM((nq + 2 * nk, DX), BF16),
                pltpu.VMEM((Z, PZ, DX), BF16),
                dma((5,)),
                *pair(Z), *pair(X), *pair(X), *pair(X), *pair(X), *pair(Z),
                *pair(X), *pair(X), *pair(Y * C), *pair(Z), *pair(Z), *pair(X, Z),
            ],
            compiler_params=pltpu.CompilerParams(
                collective_id=0, has_side_effects=True, vmem_limit_bytes=60 * 1024 * 1024
            ),
            name="attention_backward",
        )(
            inputs, w_query, w_key, w_value, query_gain.reshape(1, -1), key_gain.reshape(1, -1),
            grad_out, jnp.asarray(rows), jnp.asarray(cols),
        )
        gw = gw.astype(F32)
        return din, gw[:nq], gw[nq : nq + nk], gw[nq + nk :]

    return body


def solution(mesh):
    Z, X, Y, C = 8, 4, mesh.shape["dp"] // 2, 2
    finer = Mesh(mesh.devices.reshape(Z, X, Y, C), ("z", "x", "y", "c"))
    sp, dp = ("z", "x"), ("y", "c")
    return jax.shard_map(
        make_body(Z, X, Y, C),
        mesh=finer,
        in_specs=(P(sp, None), P(dp, None), P(dp, None), P(dp, None), P(), P(), P(sp, dp)),
        out_specs=(P(sp, dp), P(dp, None), P(dp, None), P(dp, None)),
        check_vma=False,
    )
```

time: 348 us -> 89.9 us (0.26)
  the two profiles are of different devices: /device:TPU:16 before, /device:TPU:2 now
where the time goes in v1:
time: 89.9 us; the launch traced here: 89.7 us
  Pallas kernels  85.1 us (95%)
  local copies, waits for them, and re-layouts  3.9 us (4%)
    pallas_call x1, Pallas kernels, body(): pl.pallas_call(functools.partial(kernel, sizes), out_shape=(jax.ShapeDtyp...  85.1 us
    slice x2, local copies, waits for them, and re-layouts, body(): return (din, gw[:nq], gw[nq:nq + nk], gw[nq + nk:])  3.27 us

profile of v1, /device:TPU:2, one launch (start us, length us, event | category | flops | bytes accessed | tf_op | source)
XLA Modules:
  0.0 89.7 jit_solution(3841744122215470664)
XLA Ops:
  0.6 85.1 %attention_backward.1 = (bf16[192,128]{1,0:T(8,128)(2,1)}, bf16[256,2048]{1,0:T(8,128)(2,1)}) custom-call(bf16[192,2048]{1,0:T(8,128)(2,1)} %x_ref.1, bf16[128,2048]{1,0:T(8,128)(2,1)} %wq_ref.1, bf16[64,2048]{1,0:T(8,128)(2,1)} %wk_ref.1, bf16[64,2048]{1,0:T(8,128)(2,1)} %wv_ref.1, f32[1,64]{1,0:T(1,128)} %bitcast.2, f32[1,64]{1,0:T(1,128)} %bitcast.3, ...), custom_call_target="tpu_custom_call" | custom-call | tf_op jit(solution)/shard_map/attention_backward/pallas_call | solution.py:369
  85.8 0.0 copy-start
  85.8 2.2 %slice.12 = f32[128,2048]{1,0:T(8,128)} slice(bf16[256,2048]{1,0:T(8,128)(2,1)} %get-tuple-element.7), slice={[0:128], [0:2048]} | slice | bytes 2097152 | tf_op jit(solution)/shard_map/slice | solution.py:416
  88.0 0.0 copy-done
  88.0 0.0 copy-start.1
  88.0 1.1 %fusion = (f32[64,2048]{1,0:T(8,128)}, f32[64,2048]{1,0:T(8,128)}) fusion(bf16[256,2048]{1,0:T(8,128)(2,1)S(1)} %copy-done), kind=kLoop, calls=%fused_computation | loop fusion | bytes 2097152 | tf_op jit(solution)/shard_map/slice | solution.py:416
  89.0 0.0 copy-done.1
  89.0 0.6 copy.14
Async XLA Ops:
  85.8 2.2 %copy-start = (bf16[256,2048]{1,0:T(8,128)(2,1)S(1)}, bf16[256,2048]{1,0:T(8,128)(2,1)}, u32[]{:S(2)}) copy-start(bf16[256,2048]{1,0:T(8,128)(2,1)} %get-tuple-element.7) | copy-start | bytes 3145732
  88.0 1.1 %copy-start.1 = (bf16[192,128]{1,0:T(8,128)(2,1)S(1)}, bf16[192,128]{1,0:T(8,128)(2,1)}, u32[]{:S(2)}) copy-start(bf16[192,128]{1,0:T(8,128)(2,1)} %get-tuple-element.14) | copy-start | bytes 147460

commit v2 on v1

--- a/solution.py
+++ b/solution.py
@@ -29,6 +29,10 @@
     return lax.dot_general(a, b, dims, preferred_element_type=F32)
 
 
+def mark(name):
+    pass
+
+
 def rotation_constants(grid_rows):
     quarter = HEAD_WIDTH // 4
     freqs = axial_base ** (-np.arange(quarter, dtype=np.float64) / quarter)
@@ -56,12 +60,13 @@
 def kernel(
     sizes, x_ref, wq_ref, wk_ref, wv_ref, qg_ref, kg_ref, do_ref, rows_ref, cols_ref,
     din_ref, gw_ref,
-    w_all, x_buf, kv_buf, q_buf, do_buf, qa, doa, e_buf, dp_buf, stat, cfac, delta, st_buf,
-    dqt, dq_all, dkv_send, dkv_buf, dq_send, dq_buf, g_buf, xin, hp_send, hp_buf, gw_part, gwr_buf,
+    w_all, x_buf, kv_buf, q_buf, do_buf, w_buf, e_buf, dp_buf, stat, cfac, delta, st_buf,
+    dqt, dkv_send, dkv_buf, dq_send, dq_buf, g_buf, xin, hp_send, hp_buf, gw_part, gwr_buf,
     load_sem, kv_ss, kv_rs, q_ss, q_rs, do_ss, do_rs, st_ss, st_rs, xin_ss, xin_rs, dkv_ss, dkv_rs,
     dq_ss, dq_rs, g_ss, g_rs, hp_ss, hp_rs, gwr_ss, gwr_rs, agz_ss, agz_rs, agx_ss, agx_rs,
 ):
-    Z, X, Y, C, T, D, R, CH = sizes
+    Z, X, Y, C, T, D = sizes
+    tiles = GROUP * T // LANES
     DX = D // X
     DC = D // (Y * C)
     WR = w_all.shape[0]
@@ -90,8 +95,9 @@
         pltpu.make_async_copy(wq_ref, w_all.at[pl.ds(0, nq)], load_sem.at[1]),
         pltpu.make_async_copy(wk_ref, w_all.at[pl.ds(nq, nk)], load_sem.at[2]),
         pltpu.make_async_copy(wv_ref, w_all.at[pl.ds(nq + nk, nk)], load_sem.at[3]),
-        pltpu.make_async_copy(do_ref, do_buf.at[x], load_sem.at[4]),
+        pltpu.make_async_copy(do_ref, do_buf.at[0], load_sem.at[4]),
     ]
+    mark("a_issue_loads")
     for load in loads:
         load.start()
     barrier = pltpu.get_barrier_semaphore()
@@ -131,6 +137,7 @@
         second = jnp.sum(jnp.where(head0, 0.0, v), axis=1, keepdims=True)
         return jnp.where(head0, first, second) * (1.0 / HEAD_WIDTH)
 
+    mark("b_proj")
     qg = jnp.concatenate([qg_ref[...], qg_ref[...]], axis=1)
     kg = jnp.concatenate([kg_ref[...], kg_ref[...]], axis=1)
 
@@ -143,68 +150,99 @@
     q_hat = q_raw * q_inv
     k_inv = lax.rsqrt(head_mean(kv_raw * kv_raw) + norm_eps)
     k_hat = kv_raw * k_inv
-    q_buf[x] = rotate(q_hat * qg).astype(BF16)
+    q_buf[0] = rotate(q_hat * qg).astype(BF16)
     kv_buf[0] = jnp.where(head0, rotate(k_hat * kg), kv_raw).astype(BF16)
 
+    mark("c_barrier")
     pl.semaphore_wait(barrier, (Z - 1) + (X - 1) + len(dp_pairs))
 
+    mark("d_issue")
     kv_copies, q_copies, do_copies = {}, {}, {}
     for d in nearest_first(Z):
         kv_copies[d] = remote(kv_buf.at[0], kv_buf.at[d], kv_ss.at[d], kv_rs.at[d], on_z(d))
         kv_copies[d].start()
     for d in nearest_first(X):
-        q_copies[d] = remote(q_buf.at[x], q_buf.at[x], q_ss.at[d], q_rs.at[d], on_x(d))
+        q_copies[d] = remote(q_buf.at[0], q_buf.at[d], q_ss.at[d], q_rs.at[d], on_x(d))
         q_copies[d].start()
-        do_copies[d] = remote(do_buf.at[x], do_buf.at[x], do_ss.at[d], do_rs.at[d], on_x(d))
+        do_copies[d] = remote(do_buf.at[0], do_buf.at[d], do_ss.at[d], do_rs.at[d], on_x(d))
         do_copies[d].start()
-    for d in range(1, X):
-        q_copies[d].wait()
-        do_copies[d].wait()
-
-    q_rows = q_buf[...].reshape(X * T, LANES).astype(F32) * (HEAD_WIDTH**-0.5)
-    do_rows = do_buf[...].reshape(X * T, LANES).astype(F32)
-    keep = lax.broadcasted_iota(jnp.int32, (X * T, LANES), 1) < HEAD_WIDTH
-    half = R // GROUP
-    qa[0:half] = jnp.where(keep, q_rows, 0.0).astype(BF16).reshape(half, CH, LANES)
-    qa[half:] = (
-        jnp.where(keep, pltpu.roll(q_rows, HEAD_WIDTH, 1), 0.0).astype(BF16).reshape(half, CH, LANES)
-    )
-    doa[0:half] = (
-        jnp.where(keep, 0.0, pltpu.roll(do_rows, HEAD_WIDTH, 1)).astype(BF16).reshape(half, CH, LANES)
-    )
-    doa[half:] = jnp.where(keep, 0.0, do_rows).astype(BF16).reshape(half, CH, LANES)
-
-    for d in [0] + nearest_first(Z):
+
+    def src_x(d):
+        return lax.rem(x + X - d, X)
+
+    def take_queries(d):
         if d:
+            mark(f"e_qwait{d}")
+            q_copies[d].wait()
+            do_copies[d].wait()
+        mark(f"f_build{d}")
+        q_rows = q_buf[d].astype(F32) * (HEAD_WIDTH**-0.5)
+        do_rows = do_buf[d].astype(F32)
+        qa = jnp.concatenate(
+            [jnp.where(head0, q_rows, 0.0), jnp.where(head0, pltpu.roll(q_rows, HEAD_WIDTH, 1), 0.0)], axis=0
+        ).astype(BF16)
+        doa = jnp.concatenate(
+            [jnp.where(head0, 0.0, pltpu.roll(do_rows, HEAD_WIDTH, 1)), jnp.where(head0, 0.0, do_rows)], axis=0
+        ).astype(BF16)
+        for t in range(tiles):
+            w_buf[d, t, 0:LANES] = qa[t * LANES : (t + 1) * LANES]
+            w_buf[d, t, LANES:] = doa[t * LANES : (t + 1) * LANES]
+
+    def take_keys(d):
+        if d:
+            mark(f"g_kvwait{d}")
             kv_copies[d].wait()
 
-        def forward(r, carry, d=d):
-            kv = kv_buf[d]
-            s = dot(kv, qa[r], NT)
-            dp = dot(kv, doa[r], NT)
+    def forward(d, q):
+        kv = kv_buf[d]
+        for t in range(tiles):
+            both = dot(kv, w_buf[q, t], NT)
+            s = both[:, :LANES]
+            dp = both[:, LANES:]
             m = jnp.max(s, axis=0, keepdims=True)
             e = jnp.exp(s - m)
-            stat[d, 0, r] = m
-            stat[d, 1, r] = jnp.sum(e, axis=0, keepdims=True)
-            stat[d, 2, r] = jnp.sum(e * dp, axis=0, keepdims=True)
-            e_buf[d, r] = e
-            dp_buf[d, r] = dp
-            return carry
-
-        lax.fori_loop(0, R, forward, 0)
-
-    top = stat[0, 0]
-    for d in range(1, Z):
-        top = jnp.maximum(top, stat[d, 0])
-    total = jnp.zeros_like(top)
-    weighted = jnp.zeros_like(top)
-    for d in range(Z):
-        f = jnp.exp(stat[d, 0] - top)
-        total = total + stat[d, 1] * f
-        weighted = weighted + stat[d, 2] * f
-    st_buf[0, 0] = top
-    st_buf[0, 1] = total
-    st_buf[0, 2] = weighted
+            stat[d, q, t, 0] = m
+            stat[d, q, t, 1] = jnp.sum(e, axis=0, keepdims=True)
+            stat[d, q, t, 2] = jnp.sum(e * dp, axis=0, keepdims=True)
+            e_buf[d, q, t] = e
+            dp_buf[d, q, t] = dp
+
+    arrivals = []
+    zs, xs = [0] + nearest_first(Z), [0] + nearest_first(X)
+    order = [("k", 0, 0.0), ("q", 0, 0.0)]
+    order += [("k", d, 1.0 + 2.0 * min(d, Z - d) - (d < Z - d) * 0.1) for d in zs[1:]]
+    order += [("q", d, 3.5 + 3.0 * (min(d, X - d) - 1) - (d < X - d) * 0.1) for d in xs[1:]]
+    keys_in, queries_in = [], []
+    for kind, d, _ in sorted(order, key=lambda item: item[2]):
+        if kind == "k":
+            take_keys(d)
+            keys_in.append(d)
+            blocks = [(d, q) for q in queries_in]
+        else:
+            take_queries(d)
+            queries_in.append(d)
+            blocks = [(k, d) for k in keys_in]
+        if blocks:
+            mark(f"h_fwd_{kind}{d}")
+        for k, q in blocks:
+            forward(k, q)
+
+    def merged(parts):
+        top = parts[0][0]
+        for m, _, _ in parts[1:]:
+            top = jnp.maximum(top, m)
+        total, weighted = jnp.zeros_like(top), jnp.zeros_like(top)
+        for m, l, w in parts:
+            f = jnp.exp(m - top)
+            total = total + l * f
+            weighted = weighted + w * f
+        return top, total, weighted
+
+    mark("i_stat")
+    for q in range(X):
+        parts = [[stat[d, q, :, i] for i in range(3)] for d in range(Z)]
+        for i, value in enumerate(merged(parts)):
+            st_buf[0, src_x(q), i] = value
     st_copies = {}
     for d in nearest_first(X):
         st_copies[d] = remote(st_buf.at[0], st_buf.at[d], st_ss.at[d], st_rs.at[d], on_x(d))
@@ -216,36 +254,34 @@
             x_buf.at[:, pl.ds(cols, DX)], xin.at[d], xin_ss.at[d], xin_rs.at[d], on_x(d)
         )
         xin_copies[d].start()
+    mark("j_stwait")
     for d in range(1, X):
         st_copies[d].wait()
-    top = st_buf[0, 0]
-    for d in range(1, X):
-        top = jnp.maximum(top, st_buf[d, 0])
-    total = jnp.zeros_like(top)
-    weighted = jnp.zeros_like(top)
-    for d in range(X):
-        f = jnp.exp(st_buf[d, 0] - top)
-        total = total + st_buf[d, 1] * f
-        weighted = weighted + st_buf[d, 2] * f
-    log_total = top + jnp.log(total)
-    delta[...] = weighted / total
-    for d in range(Z):
-        cfac[d] = jnp.exp(stat[d, 0] - log_total)
+    mark("k_comb")
+    for q in range(X):
+        at = src_x(q)
+        top, total, weighted = merged([[st_buf[d, at, i] for i in range(3)] for d in range(X)])
+        log_total = top + jnp.log(total)
+        delta[q] = weighted / total
+        for d in range(Z):
+            cfac[d, q] = jnp.exp(stat[d, q, :, 0] - log_total)
 
     dqt[...] = jnp.zeros_like(dqt)
     dkv_copies = {}
     dkv_own = None
     for d in farthest_first(Z) + [0]:
+        mark(f"l_bwd{d}")
         k_t = kv_buf[d].astype(F32).T[:HEAD_WIDTH].astype(BF16)
 
-        def backward(r, acc, d=d, k_t=k_t):
-            p = e_buf[d, r] * cfac[d, r]
-            ds = (p * (dp_buf[d, r] - delta[r])).astype(BF16)
-            acc = acc + dot(p.astype(BF16), doa[r], NN) + dot(ds, qa[r], NN)
-            dqt[r] += dot(k_t, ds, NN)
-            return acc
-
-        acc = lax.fori_loop(0, R, backward, jnp.zeros((T, LANES), F32))
+        acc = jnp.zeros((T, LANES), F32)
+        for q in range(X):
+            scores_grad = []
+            for t in range(tiles):
+                p = e_buf[d, q, t] * cfac[d, q, t]
+                ds = (p * (dp_buf[d, q, t] - delta[q, t])).astype(BF16)
+                scores_grad.append(ds)
+                acc = acc + dot(jnp.concatenate([ds, p.astype(BF16)], axis=1), w_buf[q, t], NN)
+            dqt[q] += dot(k_t, jnp.concatenate(scores_grad, axis=1), NN)
         if d:
             dkv_send[d] = acc.astype(BF16)
             dkv_copies[d] = remote(
@@ -255,21 +291,25 @@
         else:
             dkv_own = acc
 
-    dq_rows = jnp.concatenate(
-        [jnp.concatenate([dqt[r], dqt[half + r]], axis=0).T for r in range(half)], axis=0
-    )
-    dq_all[...] = dq_rows.reshape(X, T, LANES)
-    dq_send[...] = dq_rows.astype(BF16).reshape(X, T, LANES)
+    mark("m_dq")
     dq_copies = {}
-    for d in range(1, X):
+
+    def dq_of(q):
+        rows = dqt[q].T
+        return jnp.concatenate([rows[:T], rows[T:]], axis=1)
+
+    for d in nearest_first(X):
+        dq_send[d] = dq_of(d).astype(BF16)
         dq_copies[d] = remote(
-            dq_send.at[lax.rem(x + X - d, X)], dq_buf.at[d], dq_ss.at[d], dq_rs.at[d], on_x(X - d)
+            dq_send.at[d], dq_buf.at[d], dq_ss.at[d], dq_rs.at[d], on_x(X - d)
         )
         dq_copies[d].start()
-    dq_own = dq_all[x]
+    dq_own = dq_of(0)
+    mark("n_dqwait")
     for d in range(1, X):
         dq_copies[d].wait()
         dq_own = dq_own + dq_buf[d].astype(F32)
+    mark("o_dkvwait")
     for d in range(1, Z):
         dkv_copies[d].wait()
         dkv_own = dkv_own + dkv_buf[d].astype(F32)
@@ -278,6 +318,7 @@
         u = rotate_back(grads) * gain
         return inv * (u - normed * head_mean(u * normed))
 
+    mark("p_normback")
     grad_q = norm_back(dq_own * (HEAD_WIDTH**-0.5), q_hat, q_inv, qg)
     grad_k = norm_back(jnp.where(head0, dkv_own, 0.0), k_hat, k_inv, kg)
     grad_kv = jnp.where(head0, grad_k, dkv_own)
@@ -292,6 +333,7 @@
         j = lax.rem(y + dy, Y) * C + lax.rem(c + dc, C)
         return dot(g, w_all[:, pl.ds(pl.multiple_of(j * DC, LANES), DC)], NN).astype(BF16)
 
+    mark("q_hp")
     hp_copies = {}
     for dy, dc in reversed(dp_pairs):
         slot = dy * C + dc
@@ -302,6 +344,7 @@
         hp_copies[slot].start()
     din = part_for(0, 0).astype(F32)
 
+    mark("r_gw")
     cols = pl.multiple_of(x * DX, LANES)
     gw = dot(g, x_buf[:, pl.ds(cols, DX)], TN)
     for d in range(1, X):
@@ -316,6 +359,7 @@
             gw_part.at[pl.ds(rows, PZ)], gwr_buf.at[d], gwr_ss.at[d], gwr_rs.at[d], on_z(d)
         )
         gwr_copies[d].start()
+    mark("s_gwrwait")
     my_rows = pl.multiple_of(z * PZ, PZ)
     piece = gw_part[pl.ds(my_rows, PZ), :].astype(F32)
     for d in range(1, Z):
@@ -327,6 +371,7 @@
         rows = pl.multiple_of(lax.rem(z + Z - dz, Z) * PZ, PZ)
         return gw_ref.at[pl.ds(rows, PZ), pl.ds(cols, DX)]
 
+    mark("t_agz")
     agz_copies, agx_copies = {}, {}
     own = region(0)
     for d in nearest_first(Z):
@@ -342,26 +387,34 @@
             )
             agx_copies[dz, d].start()
 
+    mark("u_hpwait")
     for slot, copy in hp_copies.items():
         copy.wait()
         din = din + hp_buf[slot].astype(F32)
     din_ref[...] = din.astype(BF16)
+    mark("v_agxwait")
     for copy in agx_copies.values():
         copy.wait()
     for copy in agz_copies.values():
         copy.wait_send()
+    mark(None)
+
+
+def widen(gw_ref, *out_refs):
+    first = 0
+    for ref in out_refs:
+        ref[...] = gw_ref[first : first + ref.shape[0]].astype(F32)
+        first += ref.shape[0]
 
 
 def make_body(Z, X, Y, C):
     def body(inputs, w_query, w_key, w_value, query_gain, key_gain, grad_out):
         T, D = inputs.shape
         nq, nk = w_query.shape[0], w_key.shape[0]
-        per_head = X * T
-        CH = 256 if per_head % 256 == 0 else 384
-        R = GROUP * per_head // CH
         rows, cols = rotation_constants(Z * X * T // GRID_W)
         DX, DC, PZ = D // X, D // (Y * C), (nq + 2 * nk) // Z
-        sizes = (Z, X, Y, C, T, D, R, CH)
+        sizes = (Z, X, Y, C, T, D)
+        tiles = GROUP * T // LANES
         dma = pltpu.SemaphoreType.DMA
         pair = lambda *n: [dma(n), dma(n)]
         vmem = pl.BlockSpec(memory_space=pltpu.VMEM)
@@ -380,16 +433,14 @@
                 pltpu.VMEM((Z, T, LANES), BF16),
                 pltpu.VMEM((X, T, LANES), BF16),
                 pltpu.VMEM((X, T, LANES), BF16),
-                pltpu.VMEM((R, CH, LANES), BF16),
-                pltpu.VMEM((R, CH, LANES), BF16),
-                pltpu.VMEM((Z, R, T, CH), F32),
-                pltpu.VMEM((Z, R, T, CH), F32),
-                pltpu.VMEM((Z, 3, R, 1, CH), F32),
-                pltpu.VMEM((Z, R, 1, CH), F32),
-                pltpu.VMEM((R, 1, CH), F32),
-                pltpu.VMEM((X, 3, R, 1, CH), F32),
-                pltpu.VMEM((R, HEAD_WIDTH, CH), F32),
-                pltpu.VMEM((X, T, LANES), F32),
+                pltpu.VMEM((X, tiles, 2 * LANES, LANES), BF16),
+                pltpu.VMEM((Z, X, tiles, T, LANES), F32),
+                pltpu.VMEM((Z, X, tiles, T, LANES), F32),
+                pltpu.VMEM((Z, X, tiles, 3, 1, LANES), F32),
+                pltpu.VMEM((Z, X, tiles, 1, LANES), F32),
+                pltpu.VMEM((X, tiles, 1, LANES), F32),
+                pltpu.VMEM((X, X, 3, tiles, 1, LANES), F32),
+                pltpu.VMEM((X, HEAD_WIDTH, GROUP * T), F32),
                 pltpu.VMEM((Z, T, LANES), BF16),
                 pltpu.VMEM((Z, T, LANES), BF16),
                 pltpu.VMEM((X, T, LANES), BF16),
@@ -412,8 +463,16 @@
             inputs, w_query, w_key, w_value, query_gain.reshape(1, -1), key_gain.reshape(1, -1),
             grad_out, jnp.asarray(rows), jnp.asarray(cols),
         )
-        gw = gw.astype(F32)
-        return din, gw[:nq], gw[nq : nq + nk], gw[nq + nk :]
+        widened = [jax.ShapeDtypeStruct((n, D), F32) for n in (nq, nk, nk)]
+        strip = D // 2
+        return din, *pl.pallas_call(
+            widen,
+            grid=(D // strip,),
+            out_shape=widened,
+            in_specs=[pl.BlockSpec((nq + 2 * nk, strip), lambda i: (0, i))],
+            out_specs=[pl.BlockSpec((n, strip), lambda i: (0, i)) for n in (nq, nk, nk)],
+            name="widen",
+        )(gw)
 
     return body
 

time: 89.9 us -> 75.6 us (0.84)
  Pallas kernels: 85.1 us -> 74.1 us
  local copies, waits for them, and re-layouts: 3.9 us -> 0.62 us
    pallas_call x1, Pallas kernels: 85.1 us -> 71.7 us  [body(): pl.pallas_call(functools.partial(kernel, sizes), out_shape=(jax.ShapeDtyp...]
    slice x2 -> x0, local copies, waits for them, and re-layouts: 3.27 us -> none  [body(): return (din, gw[:nq], gw[nq:nq + nk], gw[nq + nk:])]
    pallas_call x0 -> x1, Pallas kernels: none -> 2.4 us  [body(): pl.pallas_call(widen, grid=(D // strip,), out_shape=widened, in_specs=[pl...]
where the time goes in v2:
time: 75.6 us; the launch traced here: 75.4 us
  Pallas kernels  74.1 us (98%)
    pallas_call x1, Pallas kernels, body(): pl.pallas_call(functools.partial(kernel, sizes), out_shape=(jax.ShapeDtyp...  71.7 us
    pallas_call x1, Pallas kernels, body(): pl.pallas_call(widen, grid=(D // strip,), out_shape=widened, in_specs=[pl...  2.4 us

profile of v2, /device:TPU:2, one launch (start us, length us, event | category | flops | bytes accessed | tf_op | source)
XLA Modules:
  0.0 75.4 jit_solution(11784482093153291944)
XLA Ops:
  0.6 71.7 %attention_backward.1 = (bf16[192,128]{1,0:T(8,128)(2,1)}, bf16[256,2048]{1,0:T(8,128)(2,1)}) custom-call(bf16[192,2048]{1,0:T(8,128)(2,1)} %x_ref.1, bf16[128,2048]{1,0:T(8,128)(2,1)} %wq_ref.1, bf16[64,2048]{1,0:T(8,128)(2,1)} %wk_ref.1, bf16[64,2048]{1,0:T(8,128)(2,1)} %wv_ref.1, f32[1,64]{1,0:T(1,128)} %bitcast.2, f32[1,64]{1,0:T(1,128)} %bitcast.3, ...), custom_call_target="tpu_custom_call" | custom-call | tf_op jit(solution)/shard_map/attention_backward/pallas_call | solution.py:422
  72.4 0.0 copy-start
  72.4 2.4 %widen.1 = (f32[128,2048]{1,0:T(8,128)}, f32[64,2048]{1,0:T(8,128)}, f32[64,2048]{1,0:T(8,128)}) custom-call(bf16[256,2048]{1,0:T(8,128)(2,1)} %get-tuple-element.10.gw_ref), custom_call_target="tpu_custom_call" | custom-call | tf_op jit(solution)/shard_map/widen/pallas_call | solution.py:468
  74.8 0.0 copy-done
  74.8 0.6 copy.14
Async XLA Ops:
  72.4 2.4 %copy-start = (bf16[192,128]{1,0:T(8,128)(2,1)S(1)}, bf16[192,128]{1,0:T(8,128)(2,1)}, u32[]{:S(2)}) copy-start(bf16[192,128]{1,0:T(8,128)(2,1)} %get-tuple-element.18) | copy-start | bytes 147460

commit v3 on v2

--- a/solution.py
+++ b/solution.py
@@ -12,6 +12,8 @@
 HEAD_WIDTH = 64
 GRID_W = 64
 GROUP = 2
+CHUNKS = 4
+STRIPS = 4
 LANES = 128
 MESH = pl.DeviceIdType.MESH
 F32 = jnp.float32
@@ -58,9 +60,9 @@
 
 
 def kernel(
-    sizes, x_ref, wq_ref, wk_ref, wv_ref, qg_ref, kg_ref, do_ref, rows_ref, cols_ref,
+    sizes, x_ref, wq_ref, wk_ref, wv_ref, qg_hbm, kg_hbm, do_ref, rows_hbm, cols_hbm,
     din_ref, gw_ref,
-    w_all, x_buf, kv_buf, q_buf, do_buf, w_buf, e_buf, dp_buf, stat, cfac, delta, st_buf,
+    qg_ref, kg_ref, rows_ref, cols_ref, w_all, x_buf, kv_buf, q_buf, do_buf, w_buf, e_buf, dp_buf, stat, cfac, delta, st_buf,
     dqt, dkv_send, dkv_buf, dq_send, dq_buf, g_buf, xin, hp_send, hp_buf, gw_part, gwr_buf,
     load_sem, kv_ss, kv_rs, q_ss, q_rs, do_ss, do_rs, st_ss, st_rs, xin_ss, xin_rs, dkv_ss, dkv_rs,
     dq_ss, dq_rs, g_ss, g_rs, hp_ss, hp_rs, gwr_ss, gwr_rs, agz_ss, agz_rs, agx_ss, agx_rs,
@@ -69,8 +71,7 @@
     tiles = GROUP * T // LANES
     DX = D // X
     DC = D // (Y * C)
-    WR = w_all.shape[0]
-    PZ = WR // Z
+    PZ = LANES // Z
     z, x, y, c = (lax.axis_index(a) for a in ("z", "x", "y", "c"))
 
     def on_z(d):
@@ -90,16 +91,33 @@
     dp_pairs = [(dy, dc) for dy in [0] + nearest_first(Y) for dc in range(C) if (dy, dc) != (0, 0)]
 
     nq, nk = wq_ref.shape[0], wk_ref.shape[0]
-    loads = [
-        pltpu.make_async_copy(x_ref, x_buf, load_sem.at[0]),
-        pltpu.make_async_copy(wq_ref, w_all.at[pl.ds(0, nq)], load_sem.at[1]),
-        pltpu.make_async_copy(wk_ref, w_all.at[pl.ds(nq, nk)], load_sem.at[2]),
-        pltpu.make_async_copy(wv_ref, w_all.at[pl.ds(nq + nk, nk)], load_sem.at[3]),
-        pltpu.make_async_copy(do_ref, do_buf.at[0], load_sem.at[4]),
+    chunk = D // CHUNKS
+    sems = iter(range(load_sem.shape[0]))
+
+    def load(src, dst):
+        copy = pltpu.make_async_copy(src, dst, load_sem.at[next(sems)])
+        copy.start()
+        return copy
+
+    mark("a_issue_loads")
+    chunk_loads = []
+    for i in range(CHUNKS):
+        span = pl.ds(i * chunk, chunk)
+        chunk_loads.append(
+            [
+                load(x_ref.at[:, span], x_buf.at[:, span]),
+                load(wq_ref.at[:, span], w_all.at[pl.ds(0, nq), span]),
+                load(wk_ref.at[:, span], w_all.at[pl.ds(nq, nk), span]),
+                load(wv_ref.at[:, span], w_all.at[pl.ds(nq + nk, nk), span]),
+            ]
+        )
+    small_loads = [
+        load(rows_hbm, rows_ref),
+        load(cols_hbm, cols_ref),
+        load(qg_hbm, qg_ref),
+        load(kg_hbm, kg_ref),
+        load(do_ref, do_buf.at[0]),
     ]
-    mark("a_issue_loads")
-    for load in loads:
-        load.start()
     barrier = pltpu.get_barrier_semaphore()
     for d in range(1, Z):
         pl.semaphore_signal(barrier, inc=1, device_id=on_z(d), device_id_type=MESH)
@@ -119,10 +137,6 @@
             [rows_ref[k, pl.ds(first_row + j, 1), :] + cols_ref[k] for j in range(n_rows)], axis=0
         )
 
-    cos = table(0)
-    sin = table(1)
-    sin = jnp.where(low, -sin, sin)
-
     def turned(v):
         return jnp.where(low, pltpu.roll(v, LANES - 16, 1), pltpu.roll(v, 16, 1))
 
@@ -138,34 +152,53 @@
         return jnp.where(head0, first, second) * (1.0 / HEAD_WIDTH)
 
     mark("b_proj")
+    raw = jnp.zeros((T, 2 * LANES), F32)
+    for i, group in enumerate(chunk_loads):
+        for copy in group:
+            copy.wait()
+        raw = raw + dot(x_buf[:, i * chunk : (i + 1) * chunk], w_all[:, i * chunk : (i + 1) * chunk], NT)
+    raw = raw.astype(BF16).astype(F32)
+    for copy in small_loads:
+        copy.wait()
     qg = jnp.concatenate([qg_ref[...], qg_ref[...]], axis=1)
     kg = jnp.concatenate([kg_ref[...], kg_ref[...]], axis=1)
-
-    for load in loads:
-        load.wait()
-    raw = dot(x_buf[...], w_all[...], NT).astype(BF16).astype(F32)
-    q_raw = raw[:, :LANES]
+    cos = table(0)
+    sin = table(1)
+    sin = jnp.where(low, -sin, sin)
+
     kv_raw = raw[:, LANES:]
-    q_inv = lax.rsqrt(head_mean(q_raw * q_raw) + norm_eps)
-    q_hat = q_raw * q_inv
     k_inv = lax.rsqrt(head_mean(kv_raw * kv_raw) + norm_eps)
     k_hat = kv_raw * k_inv
-    q_buf[0] = rotate(q_hat * qg).astype(BF16)
     kv_buf[0] = jnp.where(head0, rotate(k_hat * kg), kv_raw).astype(BF16)
 
     mark("c_barrier")
     pl.semaphore_wait(barrier, (Z - 1) + (X - 1) + len(dp_pairs))
 
     mark("d_issue")
-    kv_copies, q_copies, do_copies = {}, {}, {}
+    kv_copies, q_copies, do_copies, xin_copies = {}, {}, {}, {}
     for d in nearest_first(Z):
         kv_copies[d] = remote(kv_buf.at[0], kv_buf.at[d], kv_ss.at[d], kv_rs.at[d], on_z(d))
         kv_copies[d].start()
+    q_raw = raw[:, :LANES]
+    q_inv = lax.rsqrt(head_mean(q_raw * q_raw) + norm_eps)
+    q_hat = q_raw * q_inv
+    q_buf[0] = rotate(q_hat * qg).astype(BF16)
     for d in nearest_first(X):
         q_copies[d] = remote(q_buf.at[0], q_buf.at[d], q_ss.at[d], q_rs.at[d], on_x(d))
         q_copies[d].start()
         do_copies[d] = remote(do_buf.at[0], do_buf.at[d], do_ss.at[d], do_rs.at[d], on_x(d))
         do_copies[d].start()
+
+    def send_columns(d):
+        cols = pl.multiple_of(lax.rem(x + d, X) * DX, LANES)
+        xin_copies[d] = remote(
+            x_buf.at[:, pl.ds(cols, DX)], xin.at[d], xin_ss.at[d], xin_rs.at[d], on_x(d)
+        )
+        xin_copies[d].start()
+
+    near = [d for d in nearest_first(X) if min(d, X - d) == 1]
+    for d in near:
+        send_columns(d)
 
     def src_x(d):
         return lax.rem(x + X - d, X)
@@ -247,13 +280,9 @@
     for d in nearest_first(X):
         st_copies[d] = remote(st_buf.at[0], st_buf.at[d], st_ss.at[d], st_rs.at[d], on_x(d))
         st_copies[d].start()
-    xin_copies = {}
     for d in nearest_first(X):
-        cols = pl.multiple_of(lax.rem(x + d, X) * DX, LANES)
-        xin_copies[d] = remote(
-            x_buf.at[:, pl.ds(cols, DX)], xin.at[d], xin_ss.at[d], xin_rs.at[d], on_x(d)
-        )
-        xin_copies[d].start()
+        if d not in near:
+            send_columns(d)
     mark("j_stwait")
     for d in range(1, X):
         st_copies[d].wait()
@@ -305,89 +334,109 @@
         )
         dq_copies[d].start()
     dq_own = dq_of(0)
+
+    def norm_back(grads, normed, inv, gain):
+        u = rotate_back(grads) * gain
+        return inv * (u - normed * head_mean(u * normed))
+
+    g_copies = {}
+
+    def send_grads(part, value):
+        g_buf[0, part] = value
+        for d in nearest_first(X):
+            g_copies[d, part] = remote(
+                g_buf.at[0, part], g_buf.at[d, part], g_ss.at[d, part], g_rs.at[d, part], on_x(d)
+            )
+            g_copies[d, part].start()
+
     mark("n_dqwait")
     for d in range(1, X):
         dq_copies[d].wait()
         dq_own = dq_own + dq_buf[d].astype(F32)
+    mark("n_normq")
+    grad_q = norm_back(dq_own * (HEAD_WIDTH**-0.5), q_hat, q_inv, qg).astype(BF16)
+    send_grads(0, grad_q)
     mark("o_dkvwait")
     for d in range(1, Z):
         dkv_copies[d].wait()
         dkv_own = dkv_own + dkv_buf[d].astype(F32)
-
-    def norm_back(grads, normed, inv, gain):
-        u = rotate_back(grads) * gain
-        return inv * (u - normed * head_mean(u * normed))
-
-    mark("p_normback")
-    grad_q = norm_back(dq_own * (HEAD_WIDTH**-0.5), q_hat, q_inv, qg)
+    mark("p_normk")
     grad_k = norm_back(jnp.where(head0, dkv_own, 0.0), k_hat, k_inv, kg)
-    grad_kv = jnp.where(head0, grad_k, dkv_own)
-    g = jnp.concatenate([grad_q.astype(BF16), grad_kv.astype(BF16)], axis=1)
-    g_buf[0] = g
-    g_copies = {}
-    for d in nearest_first(X):
-        g_copies[d] = remote(g_buf.at[0], g_buf.at[d], g_ss.at[d], g_rs.at[d], on_x(d))
-        g_copies[d].start()
-
-    def part_for(dy, dc):
-        j = lax.rem(y + dy, Y) * C + lax.rem(c + dc, C)
-        return dot(g, w_all[:, pl.ds(pl.multiple_of(j * DC, LANES), DC)], NN).astype(BF16)
+    grad_kv = jnp.where(head0, grad_k, dkv_own).astype(BF16)
+    send_grads(1, grad_kv)
 
     mark("q_hp")
+    g = jnp.concatenate([grad_q, grad_kv], axis=1)
+    for j in range(0, Y * C, 2):
+        two = dot(g, w_all[:, j * DC : (j + 2) * DC], NN).astype(BF16)
+        hp_send[j] = two[:, :DC]
+        hp_send[j + 1] = two[:, DC:]
     hp_copies = {}
     for dy, dc in reversed(dp_pairs):
         slot = dy * C + dc
-        hp_send[slot] = part_for(dy, dc)
+        column = lax.rem(y + dy, Y) * C + lax.rem(c + dc, C)
         hp_copies[slot] = remote(
-            hp_send.at[slot], hp_buf.at[slot], hp_ss.at[slot], hp_rs.at[slot], on_dp(dy, dc)
+            hp_send.at[column], hp_buf.at[slot], hp_ss.at[slot], hp_rs.at[slot], on_dp(dy, dc)
         )
         hp_copies[slot].start()
-    din = part_for(0, 0).astype(F32)
-
-    mark("r_gw")
+
     cols = pl.multiple_of(x * DX, LANES)
-    gw = dot(g, x_buf[:, pl.ds(cols, DX)], TN)
-    for d in range(1, X):
-        g_copies[d].wait()
-        xin_copies[d].wait()
-        gw = gw + dot(g_buf[d], xin[d], TN)
-    gw_part[...] = gw.astype(BF16)
-    gwr_copies = {}
-    for d in farthest_first(Z):
-        rows = pl.multiple_of(lax.rem(z + d, Z) * PZ, PZ)
-        gwr_copies[d] = remote(
-            gw_part.at[pl.ds(rows, PZ)], gwr_buf.at[d], gwr_ss.at[d], gwr_rs.at[d], on_z(d)
-        )
-        gwr_copies[d].start()
-    mark("s_gwrwait")
-    my_rows = pl.multiple_of(z * PZ, PZ)
-    piece = gw_part[pl.ds(my_rows, PZ), :].astype(F32)
-    for d in range(1, Z):
-        gwr_copies[d].wait()
-        piece = piece + gwr_buf[d].astype(F32)
-    gw_ref[pl.ds(my_rows, PZ), pl.ds(cols, DX)] = piece.astype(BF16)
-
-    def region(dz):
-        rows = pl.multiple_of(lax.rem(z + Z - dz, Z) * PZ, PZ)
+    gwr_copies, agz_copies, agx_copies = {}, {}, {}
+
+    def multiply(part):
+        gw = dot(g_buf[0, part], x_buf[:, pl.ds(cols, DX)], TN)
+        for d in nearest_first(X):
+            g_copies[d, part].wait()
+            if not part:
+                xin_copies[d].wait()
+            gw = gw + dot(g_buf[d, part], xin[d], TN)
+        gw_part[part] = gw.astype(BF16)
+        for d in farthest_first(Z):
+            rows = pl.multiple_of(lax.rem(z + d, Z) * PZ, PZ)
+            gwr_copies[d, part] = remote(
+                gw_part.at[part, pl.ds(rows, PZ)], gwr_buf.at[part, d],
+                gwr_ss.at[d, part], gwr_rs.at[d, part], on_z(d),
+            )
+            gwr_copies[d, part].start()
+
+    def region(part, dz):
+        rows = pl.multiple_of(part * LANES + lax.rem(z + Z - dz, Z) * PZ, PZ)
         return gw_ref.at[pl.ds(rows, PZ), pl.ds(cols, DX)]
 
-    mark("t_agz")
-    agz_copies, agx_copies = {}, {}
-    own = region(0)
-    for d in nearest_first(Z):
-        agz_copies[d] = remote(own, own, agz_ss.at[d], agz_rs.at[d], on_z(d))
-        agz_copies[d].start()
-    for dz in [0] + nearest_first(Z):
-        if dz:
-            agz_copies[dz].wait_recv()
-        block = region(dz)
+    def pass_on(part, dz):
+        block = region(part, dz)
         for d in nearest_first(X):
-            agx_copies[dz, d] = remote(
-                block, block, agx_ss.at[d, dz], agx_rs.at[d, dz], on_x(d)
-            )
-            agx_copies[dz, d].start()
+            copy = remote(block, block, agx_ss.at[d, dz, part], agx_rs.at[d, dz, part], on_x(d))
+            copy.start()
+            agx_copies[part, dz, d] = copy
+
+    def add_up(part):
+        my_rows = pl.multiple_of(z * PZ, PZ)
+        piece = gw_part[part, pl.ds(my_rows, PZ), :].astype(F32)
+        for d in farthest_first(Z):
+            gwr_copies[d, part].wait()
+            piece = piece + gwr_buf[part, d].astype(F32)
+        gw_ref[pl.ds(pl.multiple_of(part * LANES + my_rows, PZ), PZ), pl.ds(cols, DX)] = piece.astype(BF16)
+        own = region(part, 0)
+        for d in farthest_first(Z):
+            agz_copies[part, d] = remote(own, own, agz_ss.at[d, part], agz_rs.at[d, part], on_z(d))
+            agz_copies[part, d].start()
+        pass_on(part, 0)
+
+    for part in range(2):
+        mark(f"r_gw{part}")
+        multiply(part)
+    for part in range(2):
+        mark(f"s_gwrwait{part}")
+        add_up(part)
+    for part in range(2):
+        mark(f"t_agz{part}")
+        for dz in nearest_first(Z):
+            agz_copies[part, dz].wait_recv()
+            pass_on(part, dz)
 
     mark("u_hpwait")
+    din = hp_send[y * C + c].astype(F32)
     for slot, copy in hp_copies.items():
         copy.wait()
         din = din + hp_buf[slot].astype(F32)
@@ -400,11 +449,26 @@
     mark(None)
 
 
-def widen(gw_ref, *out_refs):
-    first = 0
-    for ref in out_refs:
-        ref[...] = gw_ref[first : first + ref.shape[0]].astype(F32)
-        first += ref.shape[0]
+def widen(gw_ref, din_ref, *refs):
+    *grad_refs, din_out, wide, sems = refs
+    last = pltpu.make_async_copy(din_ref, din_out, sems.at[STRIPS, 0])
+    last.start()
+    copies = [last]
+    strip = gw_ref.shape[1] // STRIPS
+    for i in range(STRIPS):
+        span = pl.ds(i * strip, strip)
+        wide[:, span] = gw_ref[:, span].astype(F32)
+        first = 0
+        for k, ref in enumerate(grad_refs):
+            rows = ref.shape[0]
+            copy = pltpu.make_async_copy(
+                wide.at[pl.ds(first, rows), span], ref.at[:, span], sems.at[i, k]
+            )
+            copy.start()
+            copies.append(copy)
+            first += rows
+    for copy in copies:
+        copy.wait()
 
 
 def make_body(Z, X, Y, C):
@@ -412,22 +476,26 @@
         T, D = inputs.shape
         nq, nk = w_query.shape[0], w_key.shape[0]
         rows, cols = rotation_constants(Z * X * T // GRID_W)
-        DX, DC, PZ = D // X, D // (Y * C), (nq + 2 * nk) // Z
+        DX, DC, PZ = D // X, D // (Y * C), LANES // Z
         sizes = (Z, X, Y, C, T, D)
         tiles = GROUP * T // LANES
         dma = pltpu.SemaphoreType.DMA
         pair = lambda *n: [dma(n), dma(n)]
         vmem = pl.BlockSpec(memory_space=pltpu.VMEM)
-        hbm = pl.BlockSpec(memory_space=pl.ANY)
+        hbm = pl.BlockSpec(memory_space=pltpu.HBM)
         din, gw = pl.pallas_call(
             functools.partial(kernel, sizes),
             out_shape=(
                 jax.ShapeDtypeStruct((T, DC), BF16),
                 jax.ShapeDtypeStruct((nq + 2 * nk, D), BF16),
             ),
-            in_specs=[hbm, hbm, hbm, hbm, vmem, vmem, hbm, vmem, vmem],
+            in_specs=[hbm] * 9,
             out_specs=(vmem, vmem),
             scratch_shapes=[
+                pltpu.VMEM((1, HEAD_WIDTH), F32),
+                pltpu.VMEM((1, HEAD_WIDTH), F32),
+                pltpu.VMEM(rows.shape, F32),
+                pltpu.VMEM(cols.shape, F32),
                 pltpu.VMEM((nq + 2 * nk, D), BF16),
                 pltpu.VMEM((T, D), BF16),
                 pltpu.VMEM((Z, T, LANES), BF16),
@@ -445,34 +513,40 @@
                 pltpu.VMEM((Z, T, LANES), BF16),
                 pltpu.VMEM((X, T, LANES), BF16),
                 pltpu.VMEM((X, T, LANES), BF16),
-                pltpu.VMEM((X, T, nq + 2 * nk), BF16),
+                pltpu.VMEM((X, 2, T, LANES), BF16),
                 pltpu.VMEM((X, T, DX), BF16),
                 pltpu.VMEM((Y * C, T, DC), BF16),
                 pltpu.VMEM((Y * C, T, DC), BF16),
-                pltpu.VMEM((nq + 2 * nk, DX), BF16),
-                pltpu.VMEM((Z, PZ, DX), BF16),
-                dma((5,)),
+                pltpu.VMEM((2, LANES, DX), BF16),
+                pltpu.VMEM((2, Z, PZ, DX), BF16),
+                dma((4 * CHUNKS + 5,)),
                 *pair(Z), *pair(X), *pair(X), *pair(X), *pair(X), *pair(Z),
-                *pair(X), *pair(X), *pair(Y * C), *pair(Z), *pair(Z), *pair(X, Z),
+                *pair(X), *pair(X, 2), *pair(Y * C), *pair(Z, 2), *pair(Z, 2), *pair(X, Z, 2),
             ],
             compiler_params=pltpu.CompilerParams(
-                collective_id=0, has_side_effects=True, vmem_limit_bytes=60 * 1024 * 1024
+                collective_id=0, has_side_effects=True, vmem_limit_bytes=40 * 1024 * 1024
             ),
             name="attention_backward",
         )(
-            inputs, w_query, w_key, w_value, query_gain.reshape(1, -1), key_gain.reshape(1, -1),
-            grad_out, jnp.asarray(rows), jnp.asarray(cols),
-        )
-        widened = [jax.ShapeDtypeStruct((n, D), F32) for n in (nq, nk, nk)]
-        strip = D // 2
-        return din, *pl.pallas_call(
+            *[
+                pltpu.with_memory_space_constraint(a, pltpu.HBM)
+                for a in (
+                    inputs, w_query, w_key, w_value, query_gain.reshape(1, -1),
+                    key_gain.reshape(1, -1), grad_out, jnp.asarray(rows), jnp.asarray(cols),
+                )
+            ]
+        )
+        rest = [jax.ShapeDtypeStruct((n, D), F32) for n in (nq, nk, nk)]
+        *grads, din = pl.pallas_call(
             widen,
-            grid=(D // strip,),
-            out_shape=widened,
-            in_specs=[pl.BlockSpec((nq + 2 * nk, strip), lambda i: (0, i))],
-            out_specs=[pl.BlockSpec((n, strip), lambda i: (0, i)) for n in (nq, nk, nk)],
+            out_shape=[*rest, jax.ShapeDtypeStruct((T, DC), BF16)],
+            in_specs=[vmem, vmem],
+            out_specs=[hbm] * 4,
+            scratch_shapes=[pltpu.VMEM((nq + 2 * nk, D), F32), dma((STRIPS + 1, 3))],
+            compiler_params=pltpu.CompilerParams(vmem_limit_bytes=16 * 1024 * 1024),
             name="widen",
-        )(gw)
+        )(gw, din)
+        return din, *grads
 
     return body
 

time: 75.6 us -> 71 us (0.939)
  Pallas kernels: 74.1 us -> 70.2 us
    pallas_call x1, Pallas kernels: 71.7 us -> 68.7 us  [body(): pl.pallas_call(functools.partial(kernel, sizes), out_shape=(jax.ShapeDtyp...]
    pallas_call x1, Pallas kernels: 2.4 us -> 1.47 us  [body(): pl.pallas_call(widen, out_shape=[*rest, jax.ShapeDtypeStruct((T, DC), BF1...]
where the time goes in v3:
time: 71 us; the launch traced here: 70.8 us
  Pallas kernels  70.2 us (99%)
    pallas_call x1, Pallas kernels, body(): pl.pallas_call(functools.partial(kernel, sizes), out_shape=(jax.ShapeDtyp...  68.7 us
    pallas_call x1, Pallas kernels, body(): pl.pallas_call(widen, out_shape=[*rest, jax.ShapeDtypeStruct((T, DC), BF1...  1.47 us

profile of v3, /device:TPU:2, one launch (start us, length us, event | category | flops | bytes accessed | tf_op | source)
XLA Modules:
  0.0 70.8 jit_solution(4915297490243954690)
XLA Ops:
  0.6 68.7 %attention_backward.1 = (bf16[192,128]{1,0:T(8,128)(2,1)S(1)}, bf16[256,2048]{1,0:T(8,128)(2,1)S(1)}) custom-call(bf16[192,2048]{1,0:T(8,128)(2,1)} %x_ref.1, bf16[128,2048]{1,0:T(8,128)(2,1)} %wq_ref.1, bf16[64,2048]{1,0:T(8,128)(2,1)} %wk_ref.1, bf16[64,2048]{1,0:T(8,128)(2,1)} %wv_ref.1, f32[1,64]{1,0:T(1,128)} %bitcast.2, f32[1,64]{1,0:T(1,128)} %bitcast.3, ...), custom_call_target="tpu_custom_call" | custom-call | tf_op jit(solution)/shard_map/attention_backward/pallas_call | solution.py:486
  69.4 1.5 %widen.1 = (f32[128,2048]{1,0:T(8,128)}, f32[64,2048]{1,0:T(8,128)}, f32[64,2048]{1,0:T(8,128)}, bf16[192,128]{1,0:T(8,128)(2,1)}) custom-call(bf16[256,2048]{1,0:T(8,128)(2,1)S(1)} %get-tuple-element.10.gw_ref, bf16[192,128]{1,0:T(8,128)(2,1)S(1)} %get-tuple-element.11.din_ref), custom_call_target="tpu_custom_call" | custom-call | tf_op jit(solution)/shard_map/widen/pallas_call | solution.py:540

commit v4 on v3

--- a/solution.py
+++ b/solution.py
@@ -63,7 +63,7 @@
     sizes, x_ref, wq_ref, wk_ref, wv_ref, qg_hbm, kg_hbm, do_ref, rows_hbm, cols_hbm,
     din_ref, gw_ref,
     qg_ref, kg_ref, rows_ref, cols_ref, w_all, x_buf, kv_buf, q_buf, do_buf, w_buf, e_buf, dp_buf, stat, cfac, delta, st_buf,
-    dqt, dkv_send, dkv_buf, dq_send, dq_buf, g_buf, xin, hp_send, hp_buf, gw_part, gwr_buf,
+    dqt, dkv_send, dkv_buf, dq_send, dq_buf, g_buf, xin, hp_send, hp_pair, hp_sum, hp_buf, gw_part, gwr_buf,
     load_sem, kv_ss, kv_rs, q_ss, q_rs, do_ss, do_rs, st_ss, st_rs, xin_ss, xin_rs, dkv_ss, dkv_rs,
     dq_ss, dq_rs, g_ss, g_rs, hp_ss, hp_rs, gwr_ss, gwr_rs, agz_ss, agz_rs, agx_ss, agx_rs,
 ):
@@ -80,15 +80,13 @@
     def on_x(d):
         return {"x": lax.rem(x + d, X)}
 
-    def on_dp(dy, dc):
-        return {"y": lax.rem(y + dy, Y), "c": lax.rem(c + dc, C)}
+    def on_y(d):
+        return {"y": lax.rem(y + d, Y)}
 
     def remote(src, dst, ss, rs, dev):
         return pltpu.make_async_remote_copy(
             src_ref=src, dst_ref=dst, send_sem=ss, recv_sem=rs, device_id=dev, device_id_type=MESH
         )
-
-    dp_pairs = [(dy, dc) for dy in [0] + nearest_first(Y) for dc in range(C) if (dy, dc) != (0, 0)]
 
     nq, nk = wq_ref.shape[0], wk_ref.shape[0]
     chunk = D // CHUNKS
@@ -123,8 +121,9 @@
         pl.semaphore_signal(barrier, inc=1, device_id=on_z(d), device_id_type=MESH)
     for d in range(1, X):
         pl.semaphore_signal(barrier, inc=1, device_id=on_x(d), device_id_type=MESH)
-    for dy, dc in dp_pairs:
-        pl.semaphore_signal(barrier, inc=1, device_id=on_dp(dy, dc), device_id_type=MESH)
+    for d in range(1, Y):
+        pl.semaphore_signal(barrier, inc=1, device_id=on_y(d), device_id_type=MESH)
+    pl.semaphore_signal(barrier, inc=1, device_id={"c": 1 - c}, device_id_type=MESH)
 
     lane = lax.broadcasted_iota(jnp.int32, (T, LANES), 1)
     low = lax.rem(lane, 32) < 16
@@ -172,7 +171,7 @@
     kv_buf[0] = jnp.where(head0, rotate(k_hat * kg), kv_raw).astype(BF16)
 
     mark("c_barrier")
-    pl.semaphore_wait(barrier, (Z - 1) + (X - 1) + len(dp_pairs))
+    pl.semaphore_wait(barrier, (Z - 1) + (X - 1) + (Y - 1) + 1)
 
     mark("d_issue")
     kv_copies, q_copies, do_copies, xin_copies = {}, {}, {}, {}
@@ -277,7 +276,7 @@
         for i, value in enumerate(merged(parts)):
             st_buf[0, src_x(q), i] = value
     st_copies = {}
-    for d in nearest_first(X):
+    for d in farthest_first(X):
         st_copies[d] = remote(st_buf.at[0], st_buf.at[d], st_ss.at[d], st_rs.at[d], on_x(d))
         st_copies[d].start()
     for d in nearest_first(X):
@@ -327,7 +326,7 @@
         rows = dqt[q].T
         return jnp.concatenate([rows[:T], rows[T:]], axis=1)
 
-    for d in nearest_first(X):
+    for d in farthest_first(X):
         dq_send[d] = dq_of(d).astype(BF16)
         dq_copies[d] = remote(
             dq_send.at[d], dq_buf.at[d], dq_ss.at[d], dq_rs.at[d], on_x(X - d)
@@ -343,7 +342,7 @@
 
     def send_grads(part, value):
         g_buf[0, part] = value
-        for d in nearest_first(X):
+        for d in farthest_first(X):
             g_copies[d, part] = remote(
                 g_buf.at[0, part], g_buf.at[d, part], g_ss.at[d, part], g_rs.at[d, part], on_x(d)
             )
@@ -367,18 +366,24 @@
 
     mark("q_hp")
     g = jnp.concatenate([grad_q, grad_kv], axis=1)
-    for j in range(0, Y * C, 2):
-        two = dot(g, w_all[:, j * DC : (j + 2) * DC], NN).astype(BF16)
-        hp_send[j] = two[:, :DC]
-        hp_send[j + 1] = two[:, DC:]
+    for j in range(Y):
+        two = dot(g, w_all[:, j * C * DC : (j + 1) * C * DC], NN).astype(BF16)
+        for k in range(C):
+            hp_send[k, j] = two[:, k * DC : (k + 1) * DC]
+    pair_copy = remote(hp_send.at[1 - c], hp_pair, hp_ss.at[0], hp_rs.at[0], {"c": 1 - c})
+    pair_copy.start()
     hp_copies = {}
-    for dy, dc in reversed(dp_pairs):
-        slot = dy * C + dc
-        column = lax.rem(y + dy, Y) * C + lax.rem(c + dc, C)
-        hp_copies[slot] = remote(
-            hp_send.at[column], hp_buf.at[slot], hp_ss.at[slot], hp_rs.at[slot], on_dp(dy, dc)
-        )
-        hp_copies[slot].start()
+
+    def send_parts():
+        mark("q_pair")
+        pair_copy.wait()
+        for j in range(Y):
+            hp_sum[j] = (hp_send[c, j].astype(F32) + hp_pair[j].astype(F32)).astype(BF16)
+        for d in farthest_first(Y):
+            hp_copies[d] = remote(
+                hp_sum.at[lax.rem(y + d, Y)], hp_buf.at[d], hp_ss.at[d], hp_rs.at[d], on_y(d)
+            )
+            hp_copies[d].start()
 
     cols = pl.multiple_of(x * DX, LANES)
     gwr_copies, agz_copies, agx_copies = {}, {}, {}
@@ -405,7 +410,7 @@
 
     def pass_on(part, dz):
         block = region(part, dz)
-        for d in nearest_first(X):
+        for d in farthest_first(X):
             copy = remote(block, block, agx_ss.at[d, dz, part], agx_rs.at[d, dz, part], on_x(d))
             copy.start()
             agx_copies[part, dz, d] = copy
@@ -416,7 +421,10 @@
         for d in farthest_first(Z):
             gwr_copies[d, part].wait()
             piece = piece + gwr_buf[part, d].astype(F32)
-        gw_ref[pl.ds(pl.multiple_of(part * LANES + my_rows, PZ), PZ), pl.ds(cols, DX)] = piece.astype(BF16)
+        gw_ref[
+            pl.ds(pl.multiple_of(part * LANES + my_rows, PZ), PZ),
+            pl.ds(cols, DX),
+        ] = piece.astype(BF16)
         own = region(part, 0)
         for d in farthest_first(Z):
             agz_copies[part, d] = remote(own, own, agz_ss.at[d, part], agz_rs.at[d, part], on_z(d))
@@ -426,6 +434,8 @@
     for part in range(2):
         mark(f"r_gw{part}")
         multiply(part)
+        if part == 0:
+            send_parts()
     for part in range(2):
         mark(f"s_gwrwait{part}")
         add_up(part)
@@ -434,12 +444,11 @@
         for dz in nearest_first(Z):
             agz_copies[part, dz].wait_recv()
             pass_on(part, dz)
-
     mark("u_hpwait")
-    din = hp_send[y * C + c].astype(F32)
-    for slot, copy in hp_copies.items():
+    din = hp_sum[y].astype(F32)
+    for d, copy in hp_copies.items():
         copy.wait()
-        din = din + hp_buf[slot].astype(F32)
+        din = din + hp_buf[d].astype(F32)
     din_ref[...] = din.astype(BF16)
     mark("v_agxwait")
     for copy in agx_copies.values():
@@ -515,13 +524,15 @@
                 pltpu.VMEM((X, T, LANES), BF16),
                 pltpu.VMEM((X, 2, T, LANES), BF16),
                 pltpu.VMEM((X, T, DX), BF16),
-                pltpu.VMEM((Y * C, T, DC), BF16),
-                pltpu.VMEM((Y * C, T, DC), BF16),
+                pltpu.VMEM((C, Y, T, DC), BF16),
+                pltpu.VMEM((Y, T, DC), BF16),
+                pltpu.VMEM((Y, T, DC), BF16),
+                pltpu.VMEM((Y, T, DC), BF16),
                 pltpu.VMEM((2, LANES, DX), BF16),
                 pltpu.VMEM((2, Z, PZ, DX), BF16),
                 dma((4 * CHUNKS + 5,)),
                 *pair(Z), *pair(X), *pair(X), *pair(X), *pair(X), *pair(Z),
-                *pair(X), *pair(X, 2), *pair(Y * C), *pair(Z, 2), *pair(Z, 2), *pair(X, Z, 2),
+                *pair(X), *pair(X, 2), *pair(Y), *pair(Z, 2), *pair(Z, 2), *pair(X, Z, 2),
             ],
             compiler_params=pltpu.CompilerParams(
                 collective_id=0, has_side_effects=True, vmem_limit_bytes=40 * 1024 * 1024

time: 71 us -> 69 us (0.972)
  Pallas kernels: 70.2 us -> 68.2 us
    pallas_call x1, Pallas kernels: 68.7 us -> 66.7 us  [body(): pl.pallas_call(functools.partial(kernel, sizes), out_shape=(jax.ShapeDtyp...]
where the time goes in v4:
time: 69 us; the launch traced here: 68.8 us
  Pallas kernels  68.2 us (99%)
    pallas_call x1, Pallas kernels, body(): pl.pallas_call(functools.partial(kernel, sizes), out_shape=(jax.ShapeDtyp...  66.7 us
    pallas_call x1, Pallas kernels, body(): pl.pallas_call(widen, out_shape=[*rest, jax.ShapeDtypeStruct((T, DC), BF1...  1.47 us

profile of v4, /device:TPU:2, one launch (start us, length us, event | category | flops | bytes accessed | tf_op | source)
XLA Modules:
  0.0 68.8 jit_solution(17616774070559460621)
XLA Ops:
  0.6 66.7 %attention_backward.1 = (bf16[192,128]{1,0:T(8,128)(2,1)S(1)}, bf16[256,2048]{1,0:T(8,128)(2,1)S(1)}) custom-call(bf16[192,2048]{1,0:T(8,128)(2,1)} %x_ref.1, bf16[128,2048]{1,0:T(8,128)(2,1)} %wq_ref.1, bf16[64,2048]{1,0:T(8,128)(2,1)} %wk_ref.1, bf16[64,2048]{1,0:T(8,128)(2,1)} %wv_ref.1, f32[1,64]{1,0:T(1,128)} %bitcast.2, f32[1,64]{1,0:T(1,128)} %bitcast.3, ...), custom_call_target="tpu_custom_call" | custom-call | tf_op jit(solution)/shard_map/attention_backward/pallas_call | solution.py:495
  67.4 1.5 %widen.1 = (f32[128,2048]{1,0:T(8,128)}, f32[64,2048]{1,0:T(8,128)}, f32[64,2048]{1,0:T(8,128)}, bf16[192,128]{1,0:T(8,128)(2,1)}) custom-call(bf16[256,2048]{1,0:T(8,128)(2,1)S(1)} %get-tuple-element.10.gw_ref, bf16[192,128]{1,0:T(8,128)(2,1)S(1)} %get-tuple-element.11.din_ref), custom_call_target="tpu_custom_call" | custom-call | tf_op jit(solution)/shard_map/widen/pallas_call | solution.py:551

commit v5 on v4

--- a/solution.py
+++ b/solution.py
@@ -12,7 +12,7 @@
 HEAD_WIDTH = 64
 GRID_W = 64
 GROUP = 2
-CHUNKS = 4
+CHUNKS = 2
 STRIPS = 4
 LANES = 128
 MESH = pl.DeviceIdType.MESH
@@ -88,6 +88,20 @@
             src_ref=src, dst_ref=dst, send_sem=ss, recv_sem=rs, device_id=dev, device_id_type=MESH
         )
 
+    barrier = pltpu.get_barrier_semaphore()
+    for d in range(1, Z):
+        pl.semaphore_signal(barrier, inc=1, device_id=on_z(d), device_id_type=MESH)
+    for d in range(1, X):
+        pl.semaphore_signal(barrier, inc=1, device_id=on_x(d), device_id_type=MESH)
+    for d in range(1, Y):
+        pl.semaphore_signal(barrier, inc=1, device_id=on_y(d), device_id_type=MESH)
+    pl.semaphore_signal(barrier, inc=1, device_id={"c": 1 - c}, device_id_type=MESH)
+
+    def all_landed(view, ss, rs, dev):
+        copy = remote(view, view, ss, rs, dev)
+        copy.wait_send()
+        copy.wait_recv()
+
     nq, nk = wq_ref.shape[0], wk_ref.shape[0]
     chunk = D // CHUNKS
     sems = iter(range(load_sem.shape[0]))
@@ -98,13 +112,12 @@
         return copy
 
     mark("a_issue_loads")
-    chunk_loads = []
+    kv_loads = []
     for i in range(CHUNKS):
         span = pl.ds(i * chunk, chunk)
-        chunk_loads.append(
+        kv_loads.append(
             [
                 load(x_ref.at[:, span], x_buf.at[:, span]),
-                load(wq_ref.at[:, span], w_all.at[pl.ds(0, nq), span]),
                 load(wk_ref.at[:, span], w_all.at[pl.ds(nq, nk), span]),
                 load(wv_ref.at[:, span], w_all.at[pl.ds(nq + nk, nk), span]),
             ]
@@ -114,17 +127,8 @@
         load(cols_hbm, cols_ref),
         load(qg_hbm, qg_ref),
         load(kg_hbm, kg_ref),
-        load(do_ref, do_buf.at[0]),
     ]
-    barrier = pltpu.get_barrier_semaphore()
-    for d in range(1, Z):
-        pl.semaphore_signal(barrier, inc=1, device_id=on_z(d), device_id_type=MESH)
-    for d in range(1, X):
-        pl.semaphore_signal(barrier, inc=1, device_id=on_x(d), device_id_type=MESH)
-    for d in range(1, Y):
-        pl.semaphore_signal(barrier, inc=1, device_id=on_y(d), device_id_type=MESH)
-    pl.semaphore_signal(barrier, inc=1, device_id={"c": 1 - c}, device_id_type=MESH)
-
+    late_loads = [load(wq_ref, w_all.at[pl.ds(0, nq)]), load(do_ref, do_buf.at[0])]
     lane = lax.broadcasted_iota(jnp.int32, (T, LANES), 1)
     low = lax.rem(lane, 32) < 16
     head0 = lane < HEAD_WIDTH
@@ -151,12 +155,13 @@
         return jnp.where(head0, first, second) * (1.0 / HEAD_WIDTH)
 
     mark("b_proj")
-    raw = jnp.zeros((T, 2 * LANES), F32)
-    for i, group in enumerate(chunk_loads):
+    raw = jnp.zeros((T, LANES), F32)
+    for i, group in enumerate(kv_loads):
         for copy in group:
             copy.wait()
-        raw = raw + dot(x_buf[:, i * chunk : (i + 1) * chunk], w_all[:, i * chunk : (i + 1) * chunk], NT)
-    raw = raw.astype(BF16).astype(F32)
+        span = slice(i * chunk, (i + 1) * chunk)
+        raw = raw + dot(x_buf[:, span], w_all[nq:, span], NT)
+    kv_raw = raw.astype(BF16).astype(F32)
     for copy in small_loads:
         copy.wait()
     qg = jnp.concatenate([qg_ref[...], qg_ref[...]], axis=1)
@@ -165,7 +170,6 @@
     sin = table(1)
     sin = jnp.where(low, -sin, sin)
 
-    kv_raw = raw[:, LANES:]
     k_inv = lax.rsqrt(head_mean(kv_raw * kv_raw) + norm_eps)
     k_hat = kv_raw * k_inv
     kv_buf[0] = jnp.where(head0, rotate(k_hat * kg), kv_raw).astype(BF16)
@@ -174,26 +178,27 @@
     pl.semaphore_wait(barrier, (Z - 1) + (X - 1) + (Y - 1) + 1)
 
     mark("d_issue")
-    kv_copies, q_copies, do_copies, xin_copies = {}, {}, {}, {}
+    kv_copies, q_copies, do_copies = {}, {}, {}
     for d in nearest_first(Z):
-        kv_copies[d] = remote(kv_buf.at[0], kv_buf.at[d], kv_ss.at[d], kv_rs.at[d], on_z(d))
+        kv_copies[d] = remote(kv_buf.at[0], kv_buf.at[d], kv_ss.at[0], kv_rs.at[d], on_z(d))
         kv_copies[d].start()
-    q_raw = raw[:, :LANES]
+    for copy in late_loads:
+        copy.wait()
+    q_raw = dot(x_buf[...], w_all[:nq], NT).astype(BF16).astype(F32)
     q_inv = lax.rsqrt(head_mean(q_raw * q_raw) + norm_eps)
     q_hat = q_raw * q_inv
     q_buf[0] = rotate(q_hat * qg).astype(BF16)
     for d in nearest_first(X):
-        q_copies[d] = remote(q_buf.at[0], q_buf.at[d], q_ss.at[d], q_rs.at[d], on_x(d))
+        q_copies[d] = remote(q_buf.at[0], q_buf.at[d], q_ss.at[0], q_rs.at[d], on_x(d))
         q_copies[d].start()
-        do_copies[d] = remote(do_buf.at[0], do_buf.at[d], do_ss.at[d], do_rs.at[d], on_x(d))
+        do_copies[d] = remote(do_buf.at[0], do_buf.at[d], do_ss.at[0], do_rs.at[d], on_x(d))
         do_copies[d].start()
 
     def send_columns(d):
         cols = pl.multiple_of(lax.rem(x + d, X) * DX, LANES)
-        xin_copies[d] = remote(
-            x_buf.at[:, pl.ds(cols, DX)], xin.at[d], xin_ss.at[d], xin_rs.at[d], on_x(d)
-        )
-        xin_copies[d].start()
+        remote(
+            x_buf.at[:, pl.ds(cols, DX)], xin.at[d], xin_ss.at[0], xin_rs.at[0], on_x(d)
+        ).start()
 
     near = [d for d in nearest_first(X) if min(d, X - d) == 1]
     for d in near:
@@ -205,8 +210,8 @@
     def take_queries(d):
         if d:
             mark(f"e_qwait{d}")
-            q_copies[d].wait()
-            do_copies[d].wait()
+            q_copies[d].wait_recv()
+            do_copies[d].wait_recv()
         mark(f"f_build{d}")
         q_rows = q_buf[d].astype(F32) * (HEAD_WIDTH**-0.5)
         do_rows = do_buf[d].astype(F32)
@@ -223,7 +228,7 @@
     def take_keys(d):
         if d:
             mark(f"g_kvwait{d}")
-            kv_copies[d].wait()
+            kv_copies[d].wait_recv()
 
     def forward(d, q):
         kv = kv_buf[d]
@@ -273,91 +278,92 @@
     mark("i_stat")
     for q in range(X):
         parts = [[stat[d, q, :, i] for i in range(3)] for d in range(Z)]
-        for i, value in enumerate(merged(parts)):
-            st_buf[0, src_x(q), i] = value
-    st_copies = {}
+        top, total, weighted = merged(parts)
+        st_buf[0, src_x(q), 0] = top + jnp.log(total)
+        st_buf[0, src_x(q), 1] = weighted / total
     for d in farthest_first(X):
-        st_copies[d] = remote(st_buf.at[0], st_buf.at[d], st_ss.at[d], st_rs.at[d], on_x(d))
-        st_copies[d].start()
+        remote(st_buf.at[0], st_buf.at[d], st_ss.at[0], st_rs.at[0], on_x(d)).start()
     for d in nearest_first(X):
         if d not in near:
             send_columns(d)
     mark("j_stwait")
-    for d in range(1, X):
-        st_copies[d].wait()
+    all_landed(st_buf.at[pl.ds(1, X - 1)], st_ss.at[0], st_rs.at[0], on_x(1))
     mark("k_comb")
     for q in range(X):
         at = src_x(q)
-        top, total, weighted = merged([[st_buf[d, at, i] for i in range(3)] for d in range(X)])
+        logs = [st_buf[d, at, 0] for d in range(X)]
+        top = functools.reduce(jnp.maximum, logs)
+        total, weighted = jnp.zeros_like(top), jnp.zeros_like(top)
+        for d in range(X):
+            f = jnp.exp(logs[d] - top)
+            total = total + f
+            weighted = weighted + st_buf[d, at, 1] * f
         log_total = top + jnp.log(total)
         delta[q] = weighted / total
         for d in range(Z):
             cfac[d, q] = jnp.exp(stat[d, q, :, 0] - log_total)
 
     dqt[...] = jnp.zeros_like(dqt)
-    dkv_copies = {}
-    dkv_own = None
+    dkv_own = dq_own = None
+
+    def as_rows(cols):
+        rows = cols.T
+        return jnp.concatenate([rows[:T], rows[T:]], axis=1)
+
+    def send_dq(d, cols):
+        dq_send[d] = as_rows(cols).astype(BF16)
+        remote(
+            dq_send.at[d], dq_buf.at[d], dq_ss.at[0], dq_rs.at[0], on_x(X - d)
+        ).start()
+
     for d in farthest_first(Z) + [0]:
         mark(f"l_bwd{d}")
         k_t = kv_buf[d].astype(F32).T[:HEAD_WIDTH].astype(BF16)
 
         acc = jnp.zeros((T, LANES), F32)
-        for q in range(X):
+        for q in farthest_first(X) + [0]:
             scores_grad = []
             for t in range(tiles):
                 p = e_buf[d, q, t] * cfac[d, q, t]
                 ds = (p * (dp_buf[d, q, t] - delta[q, t])).astype(BF16)
                 scores_grad.append(ds)
                 acc = acc + dot(jnp.concatenate([ds, p.astype(BF16)], axis=1), w_buf[q, t], NN)
-            dqt[q] += dot(k_t, jnp.concatenate(scores_grad, axis=1), NN)
+            term = dot(k_t, jnp.concatenate(scores_grad, axis=1), NN)
+            if d:
+                dqt[q] += term
+            elif q:
+                send_dq(q, dqt[q] + term)
+            else:
+                dq_own = as_rows(dqt[q] + term)
         if d:
             dkv_send[d] = acc.astype(BF16)
-            dkv_copies[d] = remote(
-                dkv_send.at[d], dkv_buf.at[d], dkv_ss.at[d], dkv_rs.at[d], on_z(Z - d)
-            )
-            dkv_copies[d].start()
+            remote(
+                dkv_send.at[d], dkv_buf.at[d], dkv_ss.at[0], dkv_rs.at[0], on_z(Z - d)
+            ).start()
         else:
             dkv_own = acc
-
-    mark("m_dq")
-    dq_copies = {}
-
-    def dq_of(q):
-        rows = dqt[q].T
-        return jnp.concatenate([rows[:T], rows[T:]], axis=1)
-
-    for d in farthest_first(X):
-        dq_send[d] = dq_of(d).astype(BF16)
-        dq_copies[d] = remote(
-            dq_send.at[d], dq_buf.at[d], dq_ss.at[d], dq_rs.at[d], on_x(X - d)
-        )
-        dq_copies[d].start()
-    dq_own = dq_of(0)
 
     def norm_back(grads, normed, inv, gain):
         u = rotate_back(grads) * gain
         return inv * (u - normed * head_mean(u * normed))
 
-    g_copies = {}
-
     def send_grads(part, value):
         g_buf[0, part] = value
         for d in farthest_first(X):
-            g_copies[d, part] = remote(
-                g_buf.at[0, part], g_buf.at[d, part], g_ss.at[d, part], g_rs.at[d, part], on_x(d)
-            )
-            g_copies[d, part].start()
+            remote(
+                g_buf.at[0, part], g_buf.at[d, part], g_ss.at[part], g_rs.at[part], on_x(d)
+            ).start()
 
     mark("n_dqwait")
+    all_landed(dq_buf.at[pl.ds(1, X - 1)], dq_ss.at[0], dq_rs.at[0], on_x(1))
     for d in range(1, X):
-        dq_copies[d].wait()
         dq_own = dq_own + dq_buf[d].astype(F32)
     mark("n_normq")
     grad_q = norm_back(dq_own * (HEAD_WIDTH**-0.5), q_hat, q_inv, qg).astype(BF16)
     send_grads(0, grad_q)
     mark("o_dkvwait")
+    all_landed(dkv_buf.at[pl.ds(1, Z - 1)], dkv_ss.at[0], dkv_rs.at[0], on_z(1))
     for d in range(1, Z):
-        dkv_copies[d].wait()
         dkv_own = dkv_own + dkv_buf[d].astype(F32)
     mark("p_normk")
     grad_k = norm_back(jnp.where(head0, dkv_own, 0.0), k_hat, k_inv, kg)
@@ -372,7 +378,6 @@
             hp_send[k, j] = two[:, k * DC : (k + 1) * DC]
     pair_copy = remote(hp_send.at[1 - c], hp_pair, hp_ss.at[0], hp_rs.at[0], {"c": 1 - c})
     pair_copy.start()
-    hp_copies = {}
 
     def send_parts():
         mark("q_pair")
@@ -380,29 +385,27 @@
         for j in range(Y):
             hp_sum[j] = (hp_send[c, j].astype(F32) + hp_pair[j].astype(F32)).astype(BF16)
         for d in farthest_first(Y):
-            hp_copies[d] = remote(
-                hp_sum.at[lax.rem(y + d, Y)], hp_buf.at[d], hp_ss.at[d], hp_rs.at[d], on_y(d)
-            )
-            hp_copies[d].start()
+            remote(
+                hp_sum.at[lax.rem(y + d, Y)], hp_buf.at[d], hp_ss.at[1], hp_rs.at[1], on_y(d)
+            ).start()
 
     cols = pl.multiple_of(x * DX, LANES)
-    gwr_copies, agz_copies, agx_copies = {}, {}, {}
+    agz_copies = {}
 
     def multiply(part):
         gw = dot(g_buf[0, part], x_buf[:, pl.ds(cols, DX)], TN)
-        for d in nearest_first(X):
-            g_copies[d, part].wait()
-            if not part:
-                xin_copies[d].wait()
+        all_landed(g_buf.at[pl.ds(1, X - 1), part], g_ss.at[part], g_rs.at[part], on_x(1))
+        if not part:
+            all_landed(xin.at[pl.ds(1, X - 1)], xin_ss.at[0], xin_rs.at[0], on_x(1))
+        for d in range(1, X):
             gw = gw + dot(g_buf[d, part], xin[d], TN)
         gw_part[part] = gw.astype(BF16)
         for d in farthest_first(Z):
             rows = pl.multiple_of(lax.rem(z + d, Z) * PZ, PZ)
-            gwr_copies[d, part] = remote(
+            remote(
                 gw_part.at[part, pl.ds(rows, PZ)], gwr_buf.at[part, d],
-                gwr_ss.at[d, part], gwr_rs.at[d, part], on_z(d),
-            )
-            gwr_copies[d, part].start()
+                gwr_ss.at[part], gwr_rs.at[part], on_z(d),
+            ).start()
 
     def region(part, dz):
         rows = pl.multiple_of(part * LANES + lax.rem(z + Z - dz, Z) * PZ, PZ)
@@ -411,31 +414,28 @@
     def pass_on(part, dz):
         block = region(part, dz)
         for d in farthest_first(X):
-            copy = remote(block, block, agx_ss.at[d, dz, part], agx_rs.at[d, dz, part], on_x(d))
-            copy.start()
-            agx_copies[part, dz, d] = copy
+            remote(block, block, agx_ss.at[0], agx_rs.at[0], on_x(d)).start()
 
     def add_up(part):
         my_rows = pl.multiple_of(z * PZ, PZ)
         piece = gw_part[part, pl.ds(my_rows, PZ), :].astype(F32)
-        for d in farthest_first(Z):
-            gwr_copies[d, part].wait()
+        all_landed(gwr_buf.at[part, pl.ds(1, Z - 1)], gwr_ss.at[part], gwr_rs.at[part], on_z(1))
+        for d in range(1, Z):
             piece = piece + gwr_buf[part, d].astype(F32)
         gw_ref[
             pl.ds(pl.multiple_of(part * LANES + my_rows, PZ), PZ),
             pl.ds(cols, DX),
         ] = piece.astype(BF16)
         own = region(part, 0)
-        for d in farthest_first(Z):
-            agz_copies[part, d] = remote(own, own, agz_ss.at[d, part], agz_rs.at[d, part], on_z(d))
+        for d in nearest_first(Z):
+            agz_copies[part, d] = remote(own, own, agz_ss.at[part], agz_rs.at[d, part], on_z(d))
             agz_copies[part, d].start()
         pass_on(part, 0)
 
     for part in range(2):
         mark(f"r_gw{part}")
         multiply(part)
-        if part == 0:
-            send_parts()
+    send_parts()
     for part in range(2):
         mark(f"s_gwrwait{part}")
         add_up(part)
@@ -446,15 +446,20 @@
             pass_on(part, dz)
     mark("u_hpwait")
     din = hp_sum[y].astype(F32)
-    for d, copy in hp_copies.items():
-        copy.wait()
+    all_landed(hp_buf.at[pl.ds(1, Y - 1)], hp_ss.at[1], hp_rs.at[1], on_y(1))
+    for d in range(1, Y):
         din = din + hp_buf[d].astype(F32)
     din_ref[...] = din.astype(BF16)
     mark("v_agxwait")
-    for copy in agx_copies.values():
-        copy.wait()
-    for copy in agz_copies.values():
-        copy.wait_send()
+    all_landed(gw_ref.at[:, pl.ds(0, (X - 1) * DX)], agx_ss.at[0], agx_rs.at[0], on_x(1))
+    view = kv_buf.at[pl.ds(1, Z - 1)]
+    remote(view, view, kv_ss.at[0], kv_rs.at[0], on_z(1)).wait_send()
+    for buf, ss, rs in ((q_buf, q_ss, q_rs), (do_buf, do_ss, do_rs)):
+        view = buf.at[pl.ds(1, X - 1)]
+        remote(view, view, ss.at[0], rs.at[0], on_x(1)).wait_send()
+    for part in range(2):
+        view = gwr_buf.at[part, pl.ds(1, Z - 1)]
+        remote(view, view, agz_ss.at[part], agz_rs.at[0, part], on_z(1)).wait_send()
     mark(None)
 
 
@@ -516,7 +521,7 @@
                 pltpu.VMEM((Z, X, tiles, 3, 1, LANES), F32),
                 pltpu.VMEM((Z, X, tiles, 1, LANES), F32),
                 pltpu.VMEM((X, tiles, 1, LANES), F32),
-                pltpu.VMEM((X, X, 3, tiles, 1, LANES), F32),
+                pltpu.VMEM((X, X, 2, tiles, 1, LANES), F32),
                 pltpu.VMEM((X, HEAD_WIDTH, GROUP * T), F32),
                 pltpu.VMEM((Z, T, LANES), BF16),
                 pltpu.VMEM((Z, T, LANES), BF16),
@@ -530,9 +535,9 @@
                 pltpu.VMEM((Y, T, DC), BF16),
                 pltpu.VMEM((2, LANES, DX), BF16),
                 pltpu.VMEM((2, Z, PZ, DX), BF16),
-                dma((4 * CHUNKS + 5,)),
-                *pair(Z), *pair(X), *pair(X), *pair(X), *pair(X), *pair(Z),
-                *pair(X), *pair(X, 2), *pair(Y), *pair(Z, 2), *pair(Z, 2), *pair(X, Z, 2),
+                dma((3 * CHUNKS + 6,)),
+                dma((1,)), dma((Z,)), dma((1,)), dma((X,)), dma((1,)), dma((X,)), *pair(1), *pair(1), *pair(1),
+                *pair(1), *pair(2), *pair(2), *pair(2), dma((2,)), dma((Z, 2)), *pair(1),
             ],
             compiler_params=pltpu.CompilerParams(
                 collective_id=0, has_side_effects=True, vmem_limit_bytes=40 * 1024 * 1024

time: 69 us -> 65.7 us (0.952)
  the two profiles are of different devices: /device:TPU:2 before, /device:TPU:8 now
where the time goes in v5:
time: 65.7 us; the launch traced here: 65.6 us
  Pallas kernels  65 us (99%)
    pallas_call x1, Pallas kernels, body(): pl.pallas_call(functools.partial(kernel, sizes), out_shape=(jax.ShapeDtyp...  63.5 us
    pallas_call x1, Pallas kernels, body(): pl.pallas_call(widen, out_shape=[*rest, jax.ShapeDtypeStruct((T, DC), BF1...  1.47 us

profile of v5, /device:TPU:8, one launch (start us, length us, event | category | flops | bytes accessed | tf_op | source)
XLA Modules:
  0.0 65.6 jit_solution(10853627002083676935)
XLA Ops:
  0.6 63.5 %attention_backward.1 = (bf16[192,128]{1,0:T(8,128)(2,1)S(1)}, bf16[256,2048]{1,0:T(8,128)(2,1)S(1)}) custom-call(bf16[192,2048]{1,0:T(8,128)(2,1)} %x_ref.1, bf16[128,2048]{1,0:T(8,128)(2,1)} %wq_ref.1, bf16[64,2048]{1,0:T(8,128)(2,1)} %wk_ref.1, bf16[64,2048]{1,0:T(8,128)(2,1)} %wv_ref.1, f32[1,64]{1,0:T(1,128)} %bitcast.2, f32[1,64]{1,0:T(1,128)} %bitcast.3, ...), custom_call_target="tpu_custom_call" | custom-call | tf_op jit(solution)/shard_map/attention_backward/pallas_call | solution.py:500
  64.1 1.5 %widen.1 = (f32[128,2048]{1,0:T(8,128)}, f32[64,2048]{1,0:T(8,128)}, f32[64,2048]{1,0:T(8,128)}, bf16[192,128]{1,0:T(8,128)(2,1)}) custom-call(bf16[256,2048]{1,0:T(8,128)(2,1)S(1)} %get-tuple-element.10.gw_ref, bf16[192,128]{1,0:T(8,128)(2,1)S(1)} %get-tuple-element.11.din_ref), custom_call_target="tpu_custom_call" | custom-call | tf_op jit(solution)/shard_map/widen/pallas_call | solution.py:556

commit v6 on v5

--- a/solution.py
+++ b/solution.py
@@ -182,8 +182,11 @@
     for d in nearest_first(Z):
         kv_copies[d] = remote(kv_buf.at[0], kv_buf.at[d], kv_ss.at[0], kv_rs.at[d], on_z(d))
         kv_copies[d].start()
-    for copy in late_loads:
-        copy.wait()
+    late_loads[1].wait()
+    for d in nearest_first(X):
+        do_copies[d] = remote(do_buf.at[0], do_buf.at[d], do_ss.at[0], do_rs.at[d], on_x(d))
+        do_copies[d].start()
+    late_loads[0].wait()
     q_raw = dot(x_buf[...], w_all[:nq], NT).astype(BF16).astype(F32)
     q_inv = lax.rsqrt(head_mean(q_raw * q_raw) + norm_eps)
     q_hat = q_raw * q_inv
@@ -191,8 +194,6 @@
     for d in nearest_first(X):
         q_copies[d] = remote(q_buf.at[0], q_buf.at[d], q_ss.at[0], q_rs.at[d], on_x(d))
         q_copies[d].start()
-        do_copies[d] = remote(do_buf.at[0], do_buf.at[d], do_ss.at[0], do_rs.at[d], on_x(d))
-        do_copies[d].start()
 
     def send_columns(d):
         cols = pl.multiple_of(lax.rem(x + d, X) * DX, LANES)
@@ -329,12 +330,7 @@
                 scores_grad.append(ds)
                 acc = acc + dot(jnp.concatenate([ds, p.astype(BF16)], axis=1), w_buf[q, t], NN)
             term = dot(k_t, jnp.concatenate(scores_grad, axis=1), NN)
-            if d:
-                dqt[q] += term
-            elif q:
-                send_dq(q, dqt[q] + term)
-            else:
-                dq_own = as_rows(dqt[q] + term)
+            dqt[q] += term
         if d:
             dkv_send[d] = acc.astype(BF16)
             remote(
@@ -342,6 +338,9 @@
             ).start()
         else:
             dkv_own = acc
+    for q in farthest_first(X):
+        send_dq(q, dqt[q])
+    dq_own = as_rows(dqt[0])
 
     def norm_back(grads, normed, inv, gain):
         u = rotate_back(grads) * gain

time: 65.7 us -> 65.4 us (level)
  the two profiles are of different devices: /device:TPU:8 before, /device:TPU:64 now
where the time goes in v6:
time: 65.4 us; the launch traced here: 65.3 us
  Pallas kernels  64.6 us (99%)
    pallas_call x1, Pallas kernels, body(): pl.pallas_call(functools.partial(kernel, sizes), out_shape=(jax.ShapeDtyp...  63.2 us
    pallas_call x1, Pallas kernels, body(): pl.pallas_call(widen, out_shape=[*rest, jax.ShapeDtypeStruct((T, DC), BF1...  1.47 us

profile of v6, /device:TPU:64, one launch (start us, length us, event | category | flops | bytes accessed | tf_op | source)
XLA Modules:
  0.0 65.3 jit_solution(15131358834658825839)
XLA Ops:
  0.6 63.2 %attention_backward.1 = (bf16[192,128]{1,0:T(8,128)(2,1)S(1)}, bf16[256,2048]{1,0:T(8,128)(2,1)S(1)}) custom-call(bf16[192,2048]{1,0:T(8,128)(2,1)} %x_ref.1, bf16[128,2048]{1,0:T(8,128)(2,1)} %wq_ref.1, bf16[64,2048]{1,0:T(8,128)(2,1)} %wk_ref.1, bf16[64,2048]{1,0:T(8,128)(2,1)} %wv_ref.1, f32[1,64]{1,0:T(1,128)} %bitcast.2, f32[1,64]{1,0:T(1,128)} %bitcast.3, ...), custom_call_target="tpu_custom_call" | custom-call | tf_op jit(solution)/shard_map/attention_backward/pallas_call | solution.py:499
  63.8 1.5 %widen.1 = (f32[128,2048]{1,0:T(8,128)}, f32[64,2048]{1,0:T(8,128)}, f32[64,2048]{1,0:T(8,128)}, bf16[192,128]{1,0:T(8,128)(2,1)}) custom-call(bf16[256,2048]{1,0:T(8,128)(2,1)S(1)} %get-tuple-element.10.gw_ref, bf16[192,128]{1,0:T(8,128)(2,1)S(1)} %get-tuple-element.11.din_ref), custom_call_target="tpu_custom_call" | custom-call | tf_op jit(solution)/shard_map/widen/pallas_call | solution.py:555
